TPU v7x, 512 devices: a 4x2x32 block of a 4x8x32 slice. The times are simulated.
512 devices in a mesh: grp: 2 (over y), sp: 32 (over z), tp: 8 (over x, core).
Axes of the slice: x: 4, y: 2, z: 32, core: 2. Of those that a mesh axis runs over, the one named last changes fastest.
The devices are a block of a 4x8x32 slice.
Arguments:
- layer_input: bfloat16 [4, 16384, 2048], P('grp', 'sp'), parts along dimension 0, may hold values from -6 to 6
- key_weight: bfloat16 [2048, 1024], P(None, 'tp'), may hold values from -0.125 to 0.125
- value_weight: bfloat16 [2048, 1024], P(None, 'tp'), may hold values from -0.125 to 0.125
- beta_weight: bfloat16 [2048, 8], replicated, may hold values from -0.125 to 0.125
- beta_shift: float32 [8], replicated
- decay_weight: bfloat16 [2048, 8], replicated, may hold values from -0.125 to 0.125
- decay_rate: float32 [8], replicated, may hold values from 0 to 0.05
- decay_extra: float32 [4, 16384, 8], P('grp', 'sp', 'tp'), parts along dimension 0, may hold values from -1.5 to 0
- query_new: bfloat16 [4, 1024], P('grp', 'tp'), parts along dimension 0, may hold values from -6 to 6
- gate_new: bfloat16 [4, 1024], P('grp', 'tp'), parts along dimension 0, may hold values from -6 to 6
- norm_gain: float32 [128], replicated, may hold values from 0.1 to 1.9
- out_weight: bfloat16 [8, 128, 2048], P('tp', 'sp'), may hold values from -0.1875 to 0.1875
Outputs:
- state_cache: bfloat16 [4, 8, 128, 128], P('grp', 'tp', None, 'sp'), parts along dimension 0
- read_out: float32 [4, 2048], P('grp', ('sp', 'tp')), parts along dimension 0
There are 2 independent parts, one for each index of `grp`. A program takes and returns all parts, laid end to end along the dimension named above; an argument that names none is the same for every part. Nothing has to cross between parts.
All inputs are finite; a program needn't handle non-finite values.
Results may differ from a plain program's by a relative error of at most 0.013.
Values sent between devices are 32-bit elements; how exact they have to be, the bound alone decides.
A program may use at most 64 MiB of HBM per device.

v0:
```python
import jax
import jax.numpy as jnp
from jax import lax
from jax.sharding import Mesh
from jax.sharding import PartitionSpec as P

DK = 128
BLK = 64
TP = ("tp_0", "tp_1")
SP_TP = ("sp", "tp_0", "tp_1")


epsilon = 1e-06
highest = lax.Precision.HIGHEST


def entering(shard, axis, combine, identity):
    size, here = (lax.axis_size(axis), lax.axis_index(axis))
    everything = lax.all_gather(shard, axis)
    start = jnp.broadcast_to(jnp.asarray(identity, shard.dtype), shard.shape)

    def turn(k, before):
        at = size - 1 - k
        reached = at > here
        new = combine(before, everything[at])
        return jnp.where(reached, new, before)

    return lax.fori_loop(0, size, turn, start)


def cut_along(shard, dim, size):
    lengths = shard.shape
    tiles = shard.reshape(*lengths[:dim], size, lengths[dim] // size, *lengths[dim + 1 :])
    return jnp.moveaxis(tiles, dim, 0)


def sum_at_owner(shard, axis, dim):
    tiles = cut_along(shard, dim, lax.axis_size(axis))
    arrived = lax.all_to_all(tiles, axis, split_axis=0, concat_axis=0, tiled=True)
    return arrived.sum(axis=0)


def copy_for_each(shard, axis):
    copies = jnp.broadcast_to(shard, (lax.axis_size(axis), *shard.shape))
    return lax.all_to_all(copies, axis, split_axis=0, concat_axis=0, tiled=True)


def over_copies(shard, axis):
    return copy_for_each(shard, axis).sum(axis=0)


def own_block(tiles, axes, sequence):
    lengths = [lax.axis_size(a) for a in axes]
    tiles = tiles.reshape(*lengths, *tiles.shape[1:])
    tiles = tiles.transpose(*sequence, *range(len(axes), tiles.ndim))
    tiles = tiles.reshape(-1, *tiles.shape[len(axes) :])
    for k in sequence:
        tiles = lax.psum_scatter(tiles, axes[k], scatter_dimension=0, tiled=True)
    return tiles[0]


def summed_rows(shard, axes, sequence, dim):
    size = lax.axis_size(axes)
    return own_block(cut_along(shard, dim, size), axes, sequence)


def local_map(key_rows, value_rows, beta, log_decay, span):
    seq_here, length, heads_here, head_size = key_rows.shape
    block_count = length // span
    unit_keys = key_rows * lax.rsqrt(jnp.sum(key_rows * key_rows, axis=-1, keepdims=True) + epsilon)

    def blocked(tensor):
        moved_axes = jnp.moveaxis(tensor, 2, 1)
        return moved_axes.reshape((seq_here, heads_here, block_count, span) + tensor.shape[3:])

    key_blocks = blocked(unit_keys)
    value_blocks = blocked(value_rows)
    beta_blocks = blocked(beta)
    cumulative = jnp.cumsum(blocked(log_decay), axis=-1)
    places = jnp.arange(span)
    strict = places[:, None] > places[None, :]
    weighted = key_blocks * beta_blocks[..., None]
    key_products = jnp.einsum("shnid,shnjd->shnij", weighted, key_blocks, precision=highest)
    spread = cumulative[..., :, None] - cumulative[..., None, :]
    lower_part = jnp.where(strict, key_products * jnp.exp(jnp.where(strict, spread, 0.0)), 0.0)
    system = jnp.eye(span, dtype=jnp.float32) + lower_part
    right_side = jnp.concatenate(
        [value_blocks * beta_blocks[..., None], weighted * jnp.exp(cumulative)[..., None]], axis=-1
    )
    solved = jax.scipy.linalg.solve_triangular(system, right_side, lower=True)
    value_part = solved[..., :head_size]
    key_part = solved[..., head_size:]
    carried_keys = key_blocks * jnp.exp(cumulative[..., -1:] - cumulative)[..., None]
    block_decay = jnp.exp(cumulative[..., -1])
    sequence_in = tuple(
        (jnp.moveaxis(tensor, 2, 0) for tensor in (value_part, key_part, carried_keys, block_decay))
    )
    zero_half = jnp.zeros((seq_here, heads_here, head_size, head_size), jnp.float32)

    def advance(carry_map, inputs):
        value_now, key_now, carried_now, decay_now = inputs
        mixed = jnp.einsum("shck,shkx->shcx", key_now, carry_map, precision=highest)
        written = jnp.einsum("shck,shcv->shkv", carried_now, value_now, precision=highest)
        carry_map = (
            carry_map * decay_now[..., None, None]
            - jnp.einsum("shck,shcx->shkx", carried_now, mixed, precision=highest)
            + jnp.concatenate([zero_half, written], axis=-1)
        )
        return (carry_map, None)

    identity = jnp.broadcast_to(jnp.eye(head_size, dtype=jnp.float32), zero_half.shape)
    initial = jnp.concatenate([identity, zero_half], axis=-1)
    whole_map, unused = lax.scan(advance, initial, sequence_in)
    return (whole_map[..., :head_size], whole_map[..., head_size:])


def compose(earlier, later):
    return jnp.einsum("shij,shjk->shik", earlier, later, precision=highest)


def per_device(
    layer_input,
    key_weight,
    value_weight,
    beta_weight,
    beta_shift,
    decay_weight,
    decay_rate,
    decay_extra,
    query_new,
    gate_new,
    norm_gain,
    out_weight,
):
    head_size = DK
    heads_here = key_weight.shape[1] // head_size
    seq_here, places_here, unused_width = layer_input.shape
    first_head = lax.axis_index(TP) * heads_here
    beta_cols = lax.dynamic_slice_in_dim(beta_weight, first_head, heads_here, 1)
    decay_cols = lax.dynamic_slice_in_dim(decay_weight, first_head, heads_here, 1)
    head_rates = lax.dynamic_slice_in_dim(decay_rate, first_head, heads_here, 0)
    head_shift = lax.dynamic_slice_in_dim(beta_shift, first_head, heads_here, 0)
    key_rows = jnp.dot(layer_input, key_weight, preferred_element_type=jnp.float32).astype(
        jnp.bfloat16
    )
    value_rows = jnp.dot(layer_input, value_weight, preferred_element_type=jnp.float32).astype(
        jnp.bfloat16
    )
    beta_raw = jnp.dot(layer_input, beta_cols, preferred_element_type=jnp.float32).astype(
        jnp.bfloat16
    )
    decay_raw = jnp.dot(layer_input, decay_cols, preferred_element_type=jnp.float32).astype(
        jnp.bfloat16
    )
    beta = jax.nn.sigmoid(beta_raw.astype(jnp.float32) + head_shift)
    log_decay = -head_rates * jax.nn.softplus(decay_raw.astype(jnp.float32)) + decay_extra
    linear_part, offset_part = local_map(
        key_rows.reshape(seq_here, places_here, heads_here, head_size).astype(jnp.float32),
        value_rows.reshape(seq_here, places_here, heads_here, head_size).astype(jnp.float32),
        beta,
        log_decay,
        BLK,
    )
    eye_maps = jnp.broadcast_to(jnp.eye(head_size, dtype=jnp.float32), linear_part.shape)
    column_count = head_size // lax.axis_size("sp")
    first_column = lax.axis_index("sp") * column_count
    after_maps = entering(linear_part, "sp", compose, eye_maps)
    own_term = compose(after_maps, offset_part)
    own_state = sum_at_owner(own_term, "sp", 3)
    state_cache = own_state.astype(jnp.bfloat16)
    query = query_new.reshape(seq_here, heads_here, head_size).astype(jnp.float32)
    query = (
        query
        * lax.rsqrt(jnp.sum(query * query, axis=-1, keepdims=True) + epsilon)
        * head_size ** (-0.5)
    )
    readout = jnp.einsum("shkv,shk->shv", own_state, query, precision=highest)
    squares = over_copies(jnp.sum(readout * readout, axis=-1), "sp")
    scaled = readout * lax.rsqrt(squares[..., None] / head_size + epsilon)
    gate_values = lax.dynamic_slice_in_dim(
        gate_new.reshape(seq_here, heads_here, head_size), first_column, column_count, 2
    ).astype(jnp.float32)
    gain_here = lax.dynamic_slice_in_dim(norm_gain, first_column, column_count, 0)
    normed = (scaled * gain_here * jax.nn.silu(gate_values)).astype(jnp.bfloat16)
    partial_value = jnp.einsum(
        "shc,hcd->sd", normed, out_weight, preferred_element_type=jnp.float32
    )
    summed = summed_rows(partial_value, SP_TP, (2, 0, 1), 1)
    return (state_cache, summed)


def solution(mesh):
    finer = Mesh(
        mesh.devices.reshape(mesh.shape["grp"], mesh.shape["sp"], 4, 2),
        ("grp", "sp", "tp_0", "tp_1"),
    )
    placed = (
        P("grp", "sp", None),
        P(None, TP),
        P(None, TP),
        P(),
        P(),
        P(),
        P(),
        P("grp", "sp", TP),
        P("grp", TP),
        P("grp", TP),
        P(),
        P(TP, "sp", None),
    )
    return jax.shard_map(
        per_device,
        mesh=finer,
        in_specs=placed,
        out_specs=(P("grp", TP, None, "sp"), P("grp", SP_TP)),
        check_vma=False,
    )
```

profile of v0, /device:TPU:40, one launch (start us, length us, event | category | flops | bytes accessed | tf_op | source)
XLA Modules:
  0.0 530.5 jit_solution(6173813384764459302)
XLA Ops:
  9.2 3.4 fusion.39
  13.5 3.5 fusion.37
  18.3 3.7 multiply_reduce_fusion
  24.5 78.6 %custom-call.4 = f32[2,8,1,64,64]{3,4,2,1,0:T(8,128)S(1)} custom-call(f32[2,8,1,64,64]{4,3,2,1,0:T(8,128)S(1)} %fusion.24), custom_call_target="InvertDiagBlocksLowerTriangular" | custom-call | tf_op jit(solution)/shard_map/jit(_solve_triangular)/vmap(vmap())/triangular_solve | solution.py:90
  105.0 9.2 %while.25 = (s32[]{:T(128)}, f32[2,1,128,256]{3,2,0,1:T(8,128)S(1)}, f32[8,2,1]{1,2,0:T(1,128)S(1)}, f32[8,2,1,64,128]{4,3,0,1,2:T(8,128)S(1)}, f32[8,2,1,64,128...) while((s32[]{:T(128)}, f32[2,1,128,256]{3,2,0,1:T(8,128)S(1)}, ...), condition=%wide.region_3.4_spmd, body=%wide.region_2.3_spmd.sunk | while | flops 126025728 | bytes 1574505 | solution.py:113
  115.2 165.2 %all-gather.3.cloned.1.call-done = f32[64,1,128,128]{3,2,1,0:T(8,128)} async-done(((f32[2,1,128,128]{3,2,1,0:T(8,128)}), f32[64,1,128,128]{3,2,1,0:T(8,128)}) %all-gather.3.cloned.1.call-update) | async-done | bytes 4194320 | tf_op jit(solution)/shard_map/all_gather | solution.py:19
  280.4 43.1 %while.26 = (s32[]{:T(128)}, f32[2,1,128,128]{2,3,0,1:T(8,128)S(1)}, s32[]{:T(128)}, f32[32,2,1,128,128]{4,3,1,0,2:T(8,128)}, s32[]{:T(128)}, /*index=5*/s32[]{:T(128)}, s32[]{:T(128)}, s32[]{:T(128)}) while((s32[]{:T(128)}, f32[2,1,128,128]{2,3,0,1:T(8,128)S(1)}, s32[]{:T(128)}, f32[32,2,1,128,128]{4,3,1,0,2:T(8,128)}, s32[]{:T(128)}, ...), condition=%wide.region_5.6_spmd, body=%wide.region_4.5_spmd.sunk | while | flops 50364424 | bytes 786577 | solution.py:28
  280.4 1.3 fusion.95
  281.7 1.3 fusion.95
  283.1 1.3 fusion.95
  284.4 1.3 fusion.95
  287.1 1.3 fusion.95
  288.5 1.3 fusion.95
  289.8 1.3 fusion.95
  291.2 1.3 fusion.95
  292.5 1.3 fusion.95
  293.9 1.3 fusion.95
  296.6 1.3 fusion.95
  297.9 1.3 fusion.95
  299.3 1.3 fusion.95
  300.6 1.3 fusion.95
  302.0 1.3 fusion.95
  303.3 1.3 fusion.95
  306.0 1.3 fusion.95
  324.4 12.7 %all-to-all-start = ((f32[32,2,1,128,4]{3,4,1,2,0:T(4,128)}), f32[32,2,1,128,4]{3,4,1,2,0:T(4,128)S(1)}, u32[]{:S(2)}, u32[]{:S(2)}) async-start(f32[32,2,1,128,4]{3,4,1,2,0:T(4,128)} %bitcast.139), calls=%async_computation | async-start | bytes 262144 | tf_op jit(solution)/shard_map/all_to_all | solution.py:39
  337.4 26.3 %all-to-all-done = f32[32,2,1,128,4]{3,4,1,2,0:T(4,128)S(1)} async-done(((f32[32,2,1,128,4]{3,4,1,2,0:T(4,128)}), f32[32,2,1,128,4]{3,4,1,2,0:T(4,128)S(1)}, u32[]{:S(2)}, u32[]{:S(2)}) %all-to-all-start) | async-done | bytes 131104 | tf_op jit(solution)/shard_map/all_to_all | solution.py:39
  364.5 4.8 all-to-all-start.1
  371.1 1.3 dynamic-slice.6
  373.2 17.7 %all-to-all-done.1 = f32[32,2,1]{1,2,0:T(1,128)S(1)} async-done(((f32[32,2,1]{1,2,0:T(1,128)}), f32[32,2,1]{1,2,0:T(1,128)S(1)}, u32[]{:S(2)}, u32[]{:S(2)}) %all-to-all-start.1) | async-done | bytes 288 | tf_op jit(solution)/shard_map/all_to_all | solution.py:45
  392.7 8.7 %reduce-scatter.3.cloned.1.call-done = f32[128,2,8]{2,0,1:T(8,128)} async-done(((f32[256,2,8]{2,0,1:T(8,128)}), f32[128,2,8]{2,0,1:T(8,128)}) %reduce-scatter.3.cloned.1.call-update) | async-done | bytes 8208 | tf_op jit(solution)/shard_map/reduce_scatter | solution.py:58
  401.4 110.5 %all-reduce.2 = f32[128,2,8]{2,0,1:T(8,128)S(1)} all-reduce(f32[128,2,8]{2,0,1:T(8,128)} %reduce-scatter.3.cloned.1.call-done), channel_id=4, replica_groups=mesh['grp'=2,'sp'=32,'tp_0'=4,'tp_1'=2] {'sp'}, use_global_device_ids=true, to_apply=%region_11.12.clone | all-reduce | flops 2048 | bytes 16384
  512.0 10.5 %all-reduce.3 = f32[4,2,8]{2,1,0:T(2,128)S(1)} all-reduce(f32[4,2,8]{2,1,0:T(2,128)S(1)} %copy.70), channel_id=5, replica_groups=mesh['grp'=2,'sp'=32,'tp_0'=4,'tp_1'=2] {'tp_0'}, use_global_device_ids=true, to_apply=%region_12.13.clone | all-reduce | flops 64 | bytes 512
  (150 shorter events, 44.3 us)
Async XLA Ops:
  7.2 11.1 %copy-start = (bf16[2048,128]{1,0:T(8,128)(2,1)S(1)}, bf16[2048,128]{1,0:T(8,128)(2,1)}, u32[]{:S(2)}) copy-start(bf16[2048,128]{1,0:T(8,128)(2,1)} %param.17) | copy-start | bytes 1572868
  7.2 5.5 %copy-start.3 = (f32[2,512,1]{1,2,0:T(1,128)S(1)}, f32[2,512,1]{1,2,0:T(1,128)}, u32[]{:S(2)}) copy-start(f32[2,512,1]{1,2,0:T(1,128)} %param.23) | copy-start | bytes 12292
  7.2 273.1 %all-gather.3.cloned.1.call-start = ((), (), s32[]{:S(2)}) async-start(), calls=%async_computation.4 | async-start | bytes 4325376 | tf_op jit(solution)/shard_map/all_gather | solution.py:19
  9.2 7.7 %copy-start.6 = (f32[8]{0:T(128)S(1)}, f32[8]{0:T(128)}, u32[]{:S(2)}) copy-start(f32[8]{0:T(128)} %param.20) | copy-start | bytes 100
  13.5 8.5 %copy-start.5 = (bf16[2048,128]{1,0:T(8,128)(2,1)S(1)}, bf16[2048,128]{1,0:T(8,128)(2,1)}, u32[]{:S(2)}) copy-start(bf16[2048,128]{1,0:T(8,128)(2,1)} %param.18) | copy-start | bytes 1572868
  18.3 3.7 copy-start.1
  114.3 222.9 %copy-start.4 = (bf16[2,128]{1,0:T(2,128)(2,1)S(1)}, bf16[2,128]{1,0:T(2,128)(2,1)}, u32[]{:S(2)}) copy-start(bf16[2,128]{1,0:T(2,128)(2,1)} %param.24) | copy-start | bytes 1540
  114.3 255.1 %copy-start.2 = (bf16[1,4,2048]{2,1,0:T(4,128)(2,1)S(1)}, bf16[1,4,2048]{2,1,0:T(4,128)(2,1)}, u32[]{:S(2)}) copy-start(bf16[1,4,2048]{2,1,0:T(4,128)(2,1)} %param.27) | copy-start | bytes 49156
  114.3 258.2 %copy-start.7 = (f32[128]{0:T(128)S(1)}, f32[128]{0:T(128)}, u32[]{:S(2)}) copy-start(f32[128]{0:T(128)} %param.26) | copy-start | bytes 1540
  114.3 276.6 %copy-start.8 = (bf16[2,128]{1,0:T(2,128)(2,1)S(1)}, bf16[2,128]{1,0:T(2,128)(2,1)}, u32[]{:S(2)}) copy-start(bf16[2,128]{1,0:T(2,128)(2,1)} %param.25) | copy-start | bytes 1540
  324.4 39.2 %all-to-all-start = ((f32[32,2,1,128,4]{3,4,1,2,0:T(4,128)}), f32[32,2,1,128,4]{3,4,1,2,0:T(4,128)S(1)}, u32[]{:S(2)}, u32[]{:S(2)}) async-start(f32[32,2,1,128,4]{3,4,1,2,0:T(4,128)} %bitcast.139), calls=%async_computation | async-start | bytes 262144 | tf_op jit(solution)/shard_map/all_to_all | solution.py:39
  364.5 26.3 %all-to-all-start.1 = ((f32[32,2,1]{1,2,0:T(1,128)}), f32[32,2,1]{1,2,0:T(1,128)S(1)}, u32[]{:S(2)}, u32[]{:S(2)}) async-start(f32[32,2,1]{1,2,0:T(1,128)} %broadcast_in_dim.45), calls=%async_computation.1 | async-start | bytes 32768 | tf_op jit(solution)/shard_map/all_to_all | solution.py:45
  369.3 32.1 %reduce-scatter.3.cloned.1.call-start = ((), (), s32[]{:S(2)}) async-start(), calls=%async_computation.3 | async-start | bytes 393216 | tf_op jit(solution)/shard_map/reduce_scatter | solution.py:58
Sparse Core Ops, SparseCore 0:
  115.2 165.1 all-gather.2
  392.2 9.1 reduce-scatter.2
where the time goes:
time: 531 us; the launch traced here: 530 us
  waiting for transfers between devices  218 us (41%)
  blocking collectives  121 us (23%)
  other arithmetic  81.6 us (15%)
  matrix products  64.7 us (12%)
  starting transfers between devices  17.6 us (3%)
  between operations  15.7 us (3%)
  local copies, waits for them, and re-layouts  10.2 us (2%)
    all_gather x1, waiting for transfers between devices, entering(): everything = lax.all_gather(shard, axis)  165 us
    unnamed x2, blocking collectives  121 us
    another operation x1, other arithmetic, local_map(): solved = jax.scipy.linalg.solve_triangular(system, right_side, lower=True)  78.6 us
    dot_general x33, matrix products, compose(): return jnp.einsum('shij,shjk->shik', earlier, later, precision=highest)  41.7 us
    all_to_all x1, waiting for transfers between devices, sum_at_owner(): lax.all_to_all(tiles, axis, split_axis=0, concat_axis=0, tiled=True)  26.3 us
    all_to_all x1, waiting for transfers between devices, copy_for_each(): return lax.all_to_all(copies, axis, split_axis=0, concat_axis=0, tiled=True)  17.7 us
    all_to_all x1, starting transfers between devices, sum_at_owner(): lax.all_to_all(tiles, axis, split_axis=0, concat_axis=0, tiled=True)  12.7 us
  transfers between devices with their start and end apart: 4, of which 4 were waited for; matrix products, arithmetic and copies ran while one was open for 1% of the time, Pallas kernels for 0%

commit v1 on v0

v1 whole, which is shorter than its diff:
```python
import functools

import jax
import jax.numpy as jnp
from jax import lax
from jax.experimental import pallas as pl
from jax.experimental.pallas import tpu as pltpu
from jax.sharding import PartitionSpec as P

MESH = pl.DeviceIdType.MESH
EPS = 1e-06
F32 = jnp.float32
BF16 = jnp.bfloat16
DK = 128
BLK = 128
CH = 32
HALF = DK // CH
NCH = 2 * HALF
QUAD = 4
NT = (((1,), (1,)), ((), ()))


def dot(a, b):
    return jnp.dot(a, b, preferred_element_type=F32)


def split(a):
    high = a.astype(BF16)
    return high, (a - high.astype(F32)).astype(BF16)


def left3(a):
    high, low = split(a)
    return jnp.concatenate([high, low, high], axis=1)


def right3(b):
    high, low = split(b)
    return jnp.concatenate([high, high, low], axis=0)


def left2(a):
    return jnp.concatenate(split(a), axis=1)


def dot3(a, b):
    return dot(left3(a), right3(b))


def local_body(x_hbm, wk_hbm, wv_hbm, bw_ref, dw_ref, shift_ref, rate_ref, extra_ref, ab_ref, w_buf, x_buf, kv_buf, m_buf, t_buf, y_buf, x_sem, w_sem):
    tp = lax.axis_index("tp")
    prompts, seg, width = x_hbm.shape
    rows = 256
    per = seg // rows
    chunks = prompts * per
    copies = []
    wcopies = [
        pltpu.make_async_copy(wk_hbm, w_buf.at[:, pl.ds(0, DK)], w_sem.at[0]),
        pltpu.make_async_copy(wv_hbm, w_buf.at[:, pl.ds(DK, DK)], w_sem.at[1]),
    ]
    for c in wcopies:
        c.start()
    for j in range(chunks):
        c = pltpu.make_async_copy(
            x_hbm.at[j // per, pl.ds((j % per) * rows, rows), :], x_buf.at[pl.ds(j * rows, rows), :], x_sem.at[j]
        )
        c.start()
        copies.append(c)
    wbd = jnp.concatenate([bw_ref[...], dw_ref[...]], axis=0)
    for c in wcopies:
        c.wait()
    raw = []
    for j in range(chunks):
        copies[j].wait()
        xs = x_buf[pl.ds(j * rows, rows), :]
        kv_buf[pl.ds(j * rows, rows), :] = dot(xs, w_buf[...]).astype(BF16)
        raw.append(lax.dot_general(wbd, xs, NT, preferred_element_type=F32))
    groups = prompts * seg // BLK
    gp = seg // BLK
    heads = bw_ref.shape[0]
    head_lane = lax.broadcasted_iota(jnp.int32, (2 * heads, 1), 0)
    pick_b = head_lane == tp
    pick_d = head_lane == tp + heads

    def pack(pick):
        lines = []
        for g in range(groups):
            at = g * BLK
            block = raw[at // rows][:, at % rows : at % rows + BLK]
            lines.append(jnp.sum(jnp.where(pick, block, 0.0), axis=0, keepdims=True))
        return jnp.concatenate(lines, axis=0)

    beta_raw = pack(pick_b).astype(BF16).astype(F32)
    decay_raw = pack(pick_d).astype(BF16).astype(F32)
    extra = jnp.concatenate(
        [extra_ref[g // gp, :, pl.ds((g % gp) * BLK, BLK)] for g in range(groups)], axis=0
    )
    beta = jax.nn.sigmoid(beta_raw + shift_ref[tp])
    softplus = jnp.maximum(decay_raw, 0.0) + jnp.log1p(jnp.exp(-jnp.abs(decay_raw)))
    log_decay = -rate_ref[tp] * softplus + extra
    row = lax.broadcasted_iota(jnp.int32, (BLK, BLK), 0)
    col = lax.broadcasted_iota(jnp.int32, (BLK, BLK), 1)
    upto = jnp.where(row <= col, 1.0, 0.0).astype(BF16)
    l1 = log_decay.astype(BF16)
    l2 = (log_decay - l1.astype(F32)).astype(BF16)
    l3 = (log_decay - l1.astype(F32) - l2.astype(F32)).astype(BF16)
    cum = dot(jnp.concatenate([l1, l2, l3], axis=1), jnp.concatenate([upto, upto, upto], axis=0))
    cum_t = cum.T
    beta_t = beta.T
    eye = row == col
    upper = row < col
    ident = jnp.where(eye, 1.0, 0.0)
    neu = upper & ((row >> 3) == (col >> 3))
    norms = []
    for g in range(groups):
        k = kv_buf[pl.ds(g * BLK, BLK), pl.ds(0, DK)]
        gram = lax.dot_general(k, k, NT, preferred_element_type=F32)
        diag = jnp.where(eye, gram, 0.0)
        r_row = lax.rsqrt(jnp.sum(diag, axis=0, keepdims=True) + EPS)
        r_col = lax.rsqrt(jnp.sum(diag, axis=1, keepdims=True) + EPS)
        c_row = cum[g : g + 1, :]
        c_col = cum_t[:, g : g + 1]
        scale = jnp.exp(jnp.where(upper, c_row - c_col, 0.0)) * (beta[g : g + 1, :] * r_row) * r_col
        m = jnp.where(upper, gram * scale, 0.0)
        m_buf[g] = m
        t_buf[g] = jnp.where(neu, m, 0.0)
        norms.append((r_row, r_col))
    p2 = []
    for g in range(groups):
        p = t_buf[g]
        p2.append(dot3(p, p))
    for g in range(groups):
        p = t_buf[g]
        both = dot3(p2[g], jnp.concatenate([p2[g], p], axis=1))
        y_buf[g] = both[:, :BLK]
        t_buf[g] = ident - p + p2[g] - both[:, BLK:]
    for g in range(groups):
        q = t_buf[g]
        t_buf[g] = q + dot3(q, y_buf[g])
    s = 8
    while s < BLK:
        mask = ((row // (2 * s)) == (col // (2 * s))) & ((row // s) % 2 == 0) & ((col // s) % 2 == 1)
        for g in range(groups):
            y_buf[g] = dot3(jnp.where(mask, m_buf[g], 0.0), t_buf[g])
        for g in range(groups):
            t = t_buf[g]
            t_buf[g] = t - dot3(t, y_buf[g])
        s *= 2
    for g in range(groups):
        r_row, r_col = norms[g]
        c_row = cum[g : g + 1, :]
        last = cum[g : g + 1, BLK - 1 : BLK]
        t = t_buf[g] * (jnp.exp(last - c_row) * r_row)
        b_col = beta_t[:, g : g + 1]
        e_col = jnp.exp(cum_t[:, g : g + 1]) * r_col * b_col
        k = kv_buf[pl.ds(g * BLK, BLK), pl.ds(0, DK)]
        v = kv_buf[pl.ds(g * BLK, BLK), pl.ds(DK, DK)]
        k2 = jnp.concatenate([k, k], axis=0)
        f = dot(left2(jnp.concatenate([t * e_col, t * b_col], axis=0)), k2)
        kt = k.T
        vt = v.T
        a_part = dot(jnp.concatenate([kt, kt], axis=1), jnp.concatenate(split(f[:BLK]), axis=0))
        b_part = dot(jnp.concatenate([vt, vt], axis=1), jnp.concatenate(split(f[BLK:]), axis=0))
        y_buf2 = jnp.concatenate([ident * jnp.exp(last) - a_part, b_part], axis=0)
        if g % gp == 0:
            maps = []
        maps.append(y_buf2)
        if g % gp == gp - 1:
            while len(maps) > 1:
                nexts = []
                for a in range(0, len(maps), 2):
                    early, late = maps[a], maps[a + 1]
                    prod = dot3(early, late[:DK])
                    nexts.append(jnp.concatenate([prod[:DK], prod[DK:] + late[DK:]], axis=0))
                maps = nexts
            p = g // gp
            for c in range(NCH):
                ab_ref[c, p] = maps[0][c * CH : (c + 1) * CH]


def comm_body(n, ntp, first_quad, ab_ref, q_ref, gate_ref, gain_ref, ow_ref, st_ref, ro_ref, lc_in, pc_in, lc_out, pc_out, comp, rhs, rhs2, b0_in, s_buf, st_in, nm_out, nm_in, ow_out, ow_all, ow_mat, part, tot, fin_in, lc_ss, lc_rs, pc_ss, pc_rs, b0_ss, b0_rs, st_ss, st_rs, nm_ss, nm_rs, ow_ss, ow_rs, pt_ss, pt_rs, fn_ss, fn_rs, rdy_lc, rdy_pc, rdy_b0):
    grp = lax.axis_index("grp")
    z = lax.axis_index("sp")
    tp = lax.axis_index("tp")
    last = n - 1
    prompts = ab_ref.shape[1]
    tiles = tot.shape[0]

    def dev(zz, t=None):
        return (grp, zz, tp if t is None else t)

    in_quad = z >= first_quad
    pos = lax.rem(jnp.maximum(z - first_quad, 0), QUAD)
    lc_recv = in_quad & (pos > 0)
    lc_send = in_quad & (pos < QUAD - 1)
    head = (z >= 1) & ((z < first_quad) | (in_quad & (pos == QUAD - 1)))
    pc_recv = head & (z > 1)
    pc_send = head & (z < last)
    prev_head = jnp.where(z <= first_quad - 1, z - 1, z - QUAD)
    next_head = jnp.where(z < first_quad - 1, z + 1, z + QUAD)

    bar = pltpu.get_barrier_semaphore()

    @pl.when(z == 1)
    def _():
        for zz in range(n):
            if zz != 1:
                pl.semaphore_signal(bar, inc=1, device_id=dev(zz), device_id_type=MESH)
        for k in range(1, ntp):
            pl.semaphore_signal(bar, inc=1, device_id=dev(z, lax.rem(tp + k, ntp)), device_id_type=MESH)

    @pl.when(lc_send)
    def _():
        pl.semaphore_signal(bar, inc=1, device_id=dev(z + 1), device_id_type=MESH)

    @pl.when(pc_send)
    def _():
        pl.semaphore_signal(bar, inc=1, device_id=dev(next_head), device_id_type=MESH)

    @pl.when(z != last)
    def _():
        pl.semaphore_signal(bar, inc=1, device_id=dev(last), device_id_type=MESH)

    one = jnp.int32(1)
    zero = jnp.int32(0)
    expect = (
        jnp.where(z == 1, ntp - 1, 1)
        + jnp.where(lc_recv, one, zero)
        + jnp.where(pc_recv, one, zero)
        + jnp.where(z == last, n - 1, 0)
    )
    pl.semaphore_wait(bar, expect)

    @pl.when(lc_recv)
    def _():
        pl.semaphore_signal(rdy_lc, inc=1, device_id=dev(z - 1), device_id_type=MESH)

    @pl.when(pc_recv)
    def _():
        pl.semaphore_signal(rdy_pc, inc=1, device_id=dev(prev_head), device_id_type=MESH)

    @pl.when(z == last)
    def _():
        pl.semaphore_signal(rdy_b0, inc=1, device_id=dev(0), device_id_type=MESH)

    ow = ow_ref[0].astype(F32)

    def ow_copy():
        return pltpu.make_async_remote_copy(
            src_ref=ow_out, dst_ref=ow_all.at[z], send_sem=ow_ss, recv_sem=ow_rs.at[z], device_id=dev(1), device_id_type=MESH
        )

    @pl.when(z != 1)
    def _():
        ow_out[...] = ow
        ow_copy().start()

    @pl.when(z == 1)
    def _():
        ow_all[1] = ow

    def lc_copy(src, c):
        return pltpu.make_async_remote_copy(
            src_ref=src.at[c], dst_ref=lc_in.at[c], send_sem=lc_ss.at[c], recv_sem=lc_rs.at[c], device_id=dev(z + 1), device_id_type=MESH
        )

    def pc_copy(src, c):
        return pltpu.make_async_remote_copy(
            src_ref=src.at[c], dst_ref=pc_in.at[c], send_sem=pc_ss.at[c], recv_sem=pc_rs.at[c], device_id=dev(next_head), device_id_type=MESH
        )

    def b0_copy(c):
        return pltpu.make_async_remote_copy(
            src_ref=ab_ref.at[HALF + c], dst_ref=b0_in.at[c], send_sem=b0_ss.at[c], recv_sem=b0_rs.at[c], device_id=dev(last), device_id_type=MESH
        )

    def set_rhs(dst, src):
        for p in range(prompts):
            a = jnp.concatenate([src[c, p] for c in range(HALF)], axis=0)
            dst[p] = right3(a)

    @pl.when(lc_recv)
    def _():
        set_rhs(rhs, ab_ref)

        @pl.when(lc_send)
        def _():
            pl.semaphore_wait(rdy_lc, 1)

        def step(c, carry):
            lc_copy(ab_ref, c).wait_recv()
            for p in range(prompts):
                y = dot(left3(lc_in[c, p]), rhs[p])
                y = y + jnp.where(c >= HALF, ab_ref[c, p], 0.0)
                lc_out[c, p] = y
                comp[c, p] = y

            @pl.when(lc_send)
            def _():
                lc_copy(lc_out, c).start()

            return carry

        lax.fori_loop(0, NCH, step, 0)

    @pl.when(lc_send & (pos == 0))
    def _():
        pl.semaphore_wait(rdy_lc, 1)
        for c in range(NCH):
            lc_copy(ab_ref, c).start()

    @pl.when((z == 1) & pc_send)
    def _():
        pl.semaphore_wait(rdy_pc, 1)
        for c in range(NCH):
            pc_copy(ab_ref, c).start()

    @pl.when(z == 0)
    def _():
        pl.semaphore_wait(rdy_b0, 1)
        for c in range(HALF):
            b0_copy(c).start()

    @pl.when(pc_recv)
    def _():
        @pl.when(jnp.logical_not(lc_recv))
        def _():
            for c in range(NCH):
                comp[c] = ab_ref[c]

        set_rhs(rhs2, comp)

        @pl.when(pc_send)
        def _():
            pl.semaphore_wait(rdy_pc, 1)

        def step(c, carry):
            pc_copy(ab_ref, c).wait_recv()
            for p in range(prompts):
                y = dot(left3(pc_in[c, p]), rhs2[p])
                pc_out[c, p] = y + jnp.where(c >= HALF, comp[c, p], 0.0)

            @pl.when(pc_send)
            def _():
                pc_copy(pc_out, c).start()

            return carry

        lax.fori_loop(0, NCH, step, 0)

    def st_copy(zz):
        t = zz // 2
        per = CH // 8
        return pltpu.make_async_remote_copy(
            src_ref=s_buf.at[t // per, :, pl.ds((t % per) * 8, 8), :], dst_ref=st_in, send_sem=st_ss.at[zz], recv_sem=st_rs, device_id=dev(zz), device_id_type=MESH
        )

    def nm_copy():
        return pltpu.make_async_remote_copy(
            src_ref=nm_out, dst_ref=nm_in, send_sem=nm_ss, recv_sem=nm_rs, device_id=dev(1), device_id_type=MESH
        )

    order = []
    for k in range(n):
        for zz in (k, last - 1 - k):
            if zz not in order and 0 <= zz < last:
                order.append(zz)

    @pl.when(z == last)
    def _():
        set_rhs(rhs, pc_out)
        for c in range(HALF):
            b0_copy(c).wait_recv()
        query = q_ref[...].astype(F32)
        query = query * lax.rsqrt(jnp.sum(query * query, axis=-1, keepdims=True) + EPS) * DK**-0.5
        reads = []
        for p in range(prompts):
            start = jnp.concatenate([b0_in[c, p] for c in range(HALF)], axis=0)
            fin = dot(left3(start), rhs[p])
            fin = fin + jnp.concatenate([pc_out[HALF + c, p] for c in range(HALF)], axis=0)
            for c in range(HALF):
                s_buf[c, p] = fin[c * CH : (c + 1) * CH]
            qh, ql = split(jnp.broadcast_to(query[p : p + 1], (8, DK)))
            fh, fl = split(fin)
            read = lax.dot_general(
                jnp.concatenate([qh, ql, qh], axis=1), jnp.concatenate([fh, fh, fl], axis=1), NT, preferred_element_type=F32
            )
            reads.append(read[0:1])
        for zz in order:
            st_copy(zz).start()
        read = jnp.concatenate(reads, axis=0)
        scaled = read * lax.rsqrt(jnp.mean(read * read, axis=-1, keepdims=True) + EPS)
        gate = gate_ref[...].astype(F32)
        normed = (scaled * gain_ref[...] * (gate * jax.nn.sigmoid(gate))).astype(BF16)
        nm_out[...] = normed.astype(F32)
        nm_copy().start()
        t = last // 2
        per = CH // 8
        for p in range(prompts):
            st_in[p] = s_buf[t // per, p, (t % per) * 8 : (t % per) * 8 + 8, :]

    def pt_copy(k):
        return pltpu.make_async_remote_copy(
            src_ref=part.at[tp], dst_ref=part.at[tp], send_sem=pt_ss.at[k], recv_sem=pt_rs.at[k], device_id=dev(1, lax.rem(tp + k, ntp)), device_id_type=MESH
        )

    def fin_copy(zz):
        return pltpu.make_async_remote_copy(
            src_ref=tot.at[zz // 2], dst_ref=fin_in, send_sem=fn_ss.at[zz], recv_sem=fn_rs, device_id=dev(zz), device_id_type=MESH
        )

    out_order = [0] + [zz for k in range(1, n) for zz in (1 + k, (1 - k) % n) if zz < n]
    out_order = [zz for i, zz in enumerate(out_order) if zz != 1 and zz not in out_order[:i]]

    @pl.when(z == 1)
    def _():
        for zz in range(n):
            if zz != 1:
                pltpu.make_async_remote_copy(
                    src_ref=ow_out, dst_ref=ow_all.at[zz], send_sem=ow_ss, recv_sem=ow_rs.at[zz], device_id=dev(1), device_id_type=MESH
                ).wait_recv()
        lines = ow_all.shape[1]
        for r in range(lines):
            ow_mat[pl.ds(r * n, n), :] = ow_all[:, r, :].astype(BF16)
        vr = lax.broadcasted_iota(jnp.int32, (DK, DK), 0)
        vc = lax.broadcasted_iota(jnp.int32, (DK, DK), 1)
        perm = jnp.where(vc == (vr % lines) * n + vr // lines, 1.0, 0.0).astype(BF16)
        half = ow_mat.shape[1] // 4
        for h in range(4):
            ow_mat[:, pl.ds(h * half, half)] = dot(perm, ow_mat[:, pl.ds(h * half, half)]).astype(BF16)
        nm_copy().wait_recv()
        lhs = jnp.concatenate([nm_in[...], jnp.zeros((8 - prompts, DK), F32)], axis=0).astype(BF16)
        res = dot(lhs, ow_mat[...])
        for t in range(tiles):
            part[tp, t] = res[0:prompts, t * 128 : (t + 1) * 128]
        for k in range(1, ntp):
            pt_copy(k).start()
        for k in range(1, ntp):
            pltpu.make_async_remote_copy(
                src_ref=part.at[tp], dst_ref=part.at[tp], send_sem=pt_ss.at[k], recv_sem=pt_rs.at[k], device_id=dev(1, lax.rem(tp + k, ntp)), device_id_type=MESH
            ).wait_recv()
        acc = part[0]
        for k in range(1, ntp):
            acc = acc + part[k]
        tot[...] = acc
        for zz in out_order:
            fin_copy(zz).start()
        fin_in[...] = acc[0]

    @pl.when(z != last)
    def _():
        pltpu.make_async_remote_copy(
            src_ref=st_in, dst_ref=st_in, send_sem=st_ss.at[0], recv_sem=st_rs, device_id=dev(last), device_id_type=MESH
        ).wait_recv()

    odd = lax.rem(z, 2)
    for p in range(prompts):
        st_ref[p] = jnp.where(odd == 1, st_in[p, 4:8, :], st_in[p, 0:4, :]).astype(BF16)

    @pl.when(z != 1)
    def _():
        pltpu.make_async_remote_copy(
            src_ref=fin_in, dst_ref=fin_in, send_sem=fn_ss.at[0], recv_sem=fn_rs, device_id=dev(1), device_id_type=MESH
        ).wait_recv()

    span = ro_ref.shape[1]
    first = odd * (ntp * span) + tp * span
    value = fin_in[...]
    lane = lax.broadcasted_iota(jnp.int32, (128, span), 0)
    want = lax.broadcasted_iota(jnp.int32, (128, span), 1) + first
    v1, v2 = split(value)
    v3 = (value - v1.astype(F32) - v2.astype(F32)).astype(BF16)
    sel = jnp.where(lane == want, 1.0, 0.0).astype(BF16)
    ro_ref[...] = dot(v1, sel) + dot(v2, sel) + dot(v3, sel)

    @pl.when(z != 1)
    def _():
        ow_copy().wait_send()

    @pl.when(lc_send)
    def _():
        for c in range(NCH):
            lc_copy(lc_out, c).wait_send()

    @pl.when(pc_send)
    def _():
        for c in range(NCH):
            pc_copy(pc_out, c).wait_send()

    @pl.when(z == 0)
    def _():
        for c in range(HALF):
            b0_copy(c).wait_send()

    @pl.when(z == last)
    def _():
        for zz in range(n):
            if zz != last:
                st_copy(zz).wait_send()
        nm_copy().wait_send()

    @pl.when(z == 1)
    def _():
        for k in range(1, ntp):
            pt_copy(k).wait_send()
        for zz in range(n):
            if zz != 1:
                fin_copy(zz).wait_send()


VM = pl.BlockSpec(memory_space=pltpu.VMEM)
SM = pl.BlockSpec(memory_space=pltpu.SMEM)
ANY = pl.BlockSpec(memory_space=pl.ANY)


def local_map(x, wk, wv, bw, dw, shift, rate, extra):
    prompts, seg, width = x.shape
    total = prompts * seg
    groups = total // BLK
    chunks = total // 256
    return pl.pallas_call(
        local_body,
        name="local_map",
        out_shape=jax.ShapeDtypeStruct((NCH, prompts, CH, DK), F32),
        in_specs=[ANY, ANY, ANY, VM, VM, SM, SM, VM],
        out_specs=VM,
        scratch_shapes=[
            pltpu.VMEM((width, 2 * DK), BF16),
            pltpu.VMEM((total, width), BF16),
            pltpu.VMEM((total, 2 * DK), BF16),
            pltpu.VMEM((groups, BLK, BLK), F32),
            pltpu.VMEM((groups, BLK, BLK), F32),
            pltpu.VMEM((groups, BLK, BLK), F32),
            pltpu.SemaphoreType.DMA((chunks,)),
            pltpu.SemaphoreType.DMA((2,)),
        ],
    )(x, wk, wv, bw, dw, shift, rate, extra)


def exchange(n, ntp, ab, q, gate, gain, ow):
    prompts = ab.shape[1]
    width = ow.shape[2]
    lines = ow.shape[1]
    quads = 3 if n >= 32 else 1
    first_quad = n - QUAD * quads
    span = width // (n * ntp)
    tiles = width // 128
    blk = pltpu.VMEM((NCH, prompts, CH, DK), F32)
    dma = pltpu.SemaphoreType.DMA
    return pl.pallas_call(
        functools.partial(comm_body, n, ntp, first_quad),
        name="exchange",
        out_shape=(
            jax.ShapeDtypeStruct((prompts, lines, DK), BF16),
            jax.ShapeDtypeStruct((prompts, span), F32),
        ),
        in_specs=[VM] * 5,
        out_specs=(VM, VM),
        scratch_shapes=[
            blk, blk, blk, blk, blk,
            pltpu.VMEM((prompts, 3 * DK, DK), BF16),
            pltpu.VMEM((prompts, 3 * DK, DK), BF16),
            pltpu.VMEM((HALF, prompts, CH, DK), F32),
            pltpu.VMEM((HALF, prompts, CH, DK), F32),
            pltpu.VMEM((prompts, 8, DK), F32),
            pltpu.VMEM((prompts, DK), F32),
            pltpu.VMEM((prompts, DK), F32),
            pltpu.VMEM((lines, width), F32),
            pltpu.VMEM((n, lines, width), F32),
            pltpu.VMEM((n * lines, width), BF16),
            pltpu.VMEM((ntp, tiles, prompts, 128), F32),
            pltpu.VMEM((tiles, prompts, 128), F32),
            pltpu.VMEM((prompts, 128), F32),
            dma((NCH,)), dma((NCH,)), dma((NCH,)), dma((NCH,)),
            dma((HALF,)), dma((HALF,)),
            dma((n,)), dma,
            dma, dma,
            dma, dma((n,)),
            dma((ntp,)), dma((ntp,)),
            dma((n,)), dma,
            pltpu.SemaphoreType.REGULAR, pltpu.SemaphoreType.REGULAR, pltpu.SemaphoreType.REGULAR,
        ],
        compiler_params=pltpu.CompilerParams(collective_id=0, has_side_effects=True),
    )(ab, q, gate, gain, ow)


def solution(mesh):
    n, ntp = mesh.shape["sp"], mesh.shape["tp"]

    def per_device(x, wk, wv, bw, shift, dw, rate, extra, q, gate, gain, ow):
        prompts, seg, width = x.shape
        ab = local_map(x, wk, wv, bw.T, dw.T, shift, rate, extra.reshape(prompts, 1, seg))
        st, ro = exchange(n, ntp, ab, q, gate, gain.reshape(1, -1), ow)
        return jnp.transpose(st, (0, 2, 1))[:, None], ro

    placed = (
        P("grp", "sp", None),
        P(None, "tp"),
        P(None, "tp"),
        P(),
        P(),
        P(),
        P(),
        P("grp", "sp", "tp"),
        P("grp", "tp"),
        P("grp", "tp"),
        P(),
        P("tp", "sp", None),
    )
    return jax.shard_map(
        per_device,
        mesh=mesh,
        in_specs=placed,
        out_specs=(P("grp", "tp", None, "sp"), P("grp", ("sp", "tp"))),
        check_vma=False,
    )
```

time: 531 us -> 114 us (0.21)
  waiting for transfers between devices: 218 us -> 0 us
  blocking collectives: 121 us -> 0 us
  Pallas kernels: 0 us -> 110 us
  other arithmetic: 81.6 us -> 0 us
  matrix products: 64.7 us -> 0 us
  starting transfers between devices: 17.6 us -> 0 us
  between operations: 15.7 us -> 0.65 us
  local copies, waits for them, and re-layouts: 10.2 us -> 2.48 us
    all_gather x1 -> x0, waiting for transfers between devices: 165 us -> none  [entering(): everything = lax.all_gather(shard, axis)]
    unnamed x2 -> x0, blocking collectives: 121 us -> none
    pallas_call x0 -> x2, Pallas kernels: none -> 110 us  [the longest x1 98.7 us: exchange(): pl.pallas_call(functools.partial(comm_body, n, ntp, first_quad), name='ex...]
    another operation x2 -> x0, other arithmetic: 79.1 us -> none  [the longest x1 78.6 us: local_map(): solved = jax.scipy.linalg.solve_triangular(system, right_side, lower=True)]
    dot_general x64 -> x0, matrix products: 63.7 us -> none  [the longest x33 41.7 us: compose(): return jnp.einsum('shij,shjk->shik', earlier, later, precision=highest)]
    all_to_all x2 -> x0, waiting for transfers between devices: 43.9 us -> none  [the longest x1 26.3 us: sum_at_owner(): lax.all_to_all(tiles, axis, split_axis=0, concat_axis=0, tiled=True)]
    all_to_all x2 -> x0, starting transfers between devices: 17.5 us -> none  [the longest x1 12.7 us: sum_at_owner(): lax.all_to_all(tiles, axis, split_axis=0, concat_axis=0, tiled=True)]
    reduce_scatter x1 -> x0, waiting for transfers between devices: 8.74 us -> none  [own_block(): tiles = lax.psum_scatter(tiles, axes[k], scatter_dimension=0, tiled=True)]
  transfers between devices with their start and end apart: 4 -> 0, of which waited for: 4 -> 0; matrix products, arithmetic and copies ran while one was open for 1% -> 0% of each run, Pallas kernels for 0% -> 0%
where the time goes in v1:
time: 114 us; the launch traced here: 113 us
  Pallas kernels  110 us (96%)
  local copies, waits for them, and re-layouts  2.48 us (2%)
    pallas_call x1, Pallas kernels, exchange(): pl.pallas_call(functools.partial(comm_body, n, ntp, first_quad), name='ex...  98.7 us
    pallas_call x1, Pallas kernels, local_map(): pl.pallas_call(local_body, name='local_map', out_shape=jax.ShapeDtypeStru...  11.5 us
    unnamed x2, local copies, waits for them, and re-layouts  2.48 us

profile of v1, /device:TPU:40, one launch (start us, length us, event | category | flops | bytes accessed | tf_op | source)
XLA Modules:
  0.0 113.3 jit_solution(8258151134256007212)
XLA Ops:
  0.6 11.5 %local_map.1.ab_ref = f32[8,2,32,128]{3,2,1,0:T(8,128)} custom-call(bf16[2,512,2048]{2,1,0:T(8,128)(2,1)} %x_hbm.1, bf16[2048,128]{1,0:T(8,128)(2,1)} %wk_hbm.1, bf16[2048,128]{1,0:T(8,128)(2,1)} %wv_hbm.1, bf16[8,2048]{1,0:T(8,128)(2,1)} %bitcast.9, bf16[8,2048]{1,0:T(8,128)(2,1)} %bitcast.10, f32[8]{0:T(128)} %shift_ref.1, f32[8]{0:T(128)} %rate_ref.1, ...), custom_call_target="tpu_custom_call" | custom-call | tf_op jit(solution)/shard_map/local_map/pallas_call | solution.py:521
  12.1 98.7 %exchange.1 = (bf16[2,4,128]{2,1,0:T(4,128)(2,1)}, f32[2,8]{1,0:T(2,128)}) custom-call(f32[8,2,32,128]{3,2,1,0:T(8,128)} %local_map.1.ab_ref, bf16[2,128]{1,0:T(2,128)(2,1)} %q_ref.1, bf16[2,128]{1,0:T(2,128)(2,1)} %gate_ref.1, f32[1,128]{1,0:T(1,128)} %bitcast.13, bf16[1,4,2048]{2,1,0:T(4,128)(2,1)} %ow_ref.1), custom_call_target="tpu_custom_call" | custom-call | tf_op jit(solution)/shard_map/exchange/pallas_call | solution.py:550
  110.9 1.3 %copy.17 = bf16[2,1,128,4]{2,3,1,0:T(4,128)(2,1)} copy(bf16[2,1,128,4]{2,3,1,0:T(4,128)(2,1)} %bitcast.12) | data formatting | bytes 4096
  112.1 1.2 %copy.18 = f32[2,8]{1,0:T(2,128)} copy(f32[2,8]{1,0:T(2,128)} %get-tuple-element.11) | data formatting | bytes 128

commit v2 on v1

--- a/solution.py
+++ b/solution.py
@@ -13,10 +13,11 @@
 BF16 = jnp.bfloat16
 DK = 128
 BLK = 128
-CH = 32
+CH = 16
+ROWS = 256
 HALF = DK // CH
 NCH = 2 * HALF
-QUAD = 4
+GROUPS = (1, 1, 1, 1, 1, 2, 2, 2, 2, 2, 3, 3, 4, 6)
 NT = (((1,), (1,)), ((), ()))
 
 
@@ -47,25 +48,11 @@
     return dot(left3(a), right3(b))
 
 
-def local_body(x_hbm, wk_hbm, wv_hbm, bw_ref, dw_ref, shift_ref, rate_ref, extra_ref, ab_ref, w_buf, x_buf, kv_buf, m_buf, t_buf, y_buf, x_sem, w_sem):
-    tp = lax.axis_index("tp")
-    prompts, seg, width = x_hbm.shape
-    rows = 256
-    per = seg // rows
-    chunks = prompts * per
-    copies = []
-    wcopies = [
-        pltpu.make_async_copy(wk_hbm, w_buf.at[:, pl.ds(0, DK)], w_sem.at[0]),
-        pltpu.make_async_copy(wv_hbm, w_buf.at[:, pl.ds(DK, DK)], w_sem.at[1]),
-    ]
-    for c in wcopies:
-        c.start()
-    for j in range(chunks):
-        c = pltpu.make_async_copy(
-            x_hbm.at[j // per, pl.ds((j % per) * rows, rows), :], x_buf.at[pl.ds(j * rows, rows), :], x_sem.at[j]
-        )
-        c.start()
-        copies.append(c)
+def local_body(tp, prompts, seg, wcopies, copies, scopies, bw_ref, dw_ref, shift_ref, rate_ref, extra_ref, ab_ref, w_buf, x_buf, kv_buf, m_buf, t_buf, y_buf):
+    rows = ROWS
+    chunks = len(copies)
+    for c in scopies:
+        c.wait()
     wbd = jnp.concatenate([bw_ref[...], dw_ref[...]], axis=0)
     for c in wcopies:
         c.wait()
@@ -95,9 +82,12 @@
     extra = jnp.concatenate(
         [extra_ref[g // gp, :, pl.ds((g % gp) * BLK, BLK)] for g in range(groups)], axis=0
     )
-    beta = jax.nn.sigmoid(beta_raw + shift_ref[tp])
+    own = lax.broadcasted_iota(jnp.int32, (1, heads), 1) == tp
+    shift = jnp.sum(jnp.where(own, shift_ref[...], 0.0), axis=1, keepdims=True)
+    rate = jnp.sum(jnp.where(own, rate_ref[...], 0.0), axis=1, keepdims=True)
+    beta = jax.nn.sigmoid(beta_raw + shift)
     softplus = jnp.maximum(decay_raw, 0.0) + jnp.log1p(jnp.exp(-jnp.abs(decay_raw)))
-    log_decay = -rate_ref[tp] * softplus + extra
+    log_decay = -rate * softplus + extra
     row = lax.broadcasted_iota(jnp.int32, (BLK, BLK), 0)
     col = lax.broadcasted_iota(jnp.int32, (BLK, BLK), 1)
     upto = jnp.where(row <= col, 1.0, 0.0).astype(BF16)
@@ -178,36 +168,71 @@
                 ab_ref[c, p] = maps[0][c * CH : (c + 1) * CH]
 
 
-def comm_body(n, ntp, first_quad, ab_ref, q_ref, gate_ref, gain_ref, ow_ref, st_ref, ro_ref, lc_in, pc_in, lc_out, pc_out, comp, rhs, rhs2, b0_in, s_buf, st_in, nm_out, nm_in, ow_out, ow_all, ow_mat, part, tot, fin_in, lc_ss, lc_rs, pc_ss, pc_rs, b0_ss, b0_rs, st_ss, st_rs, nm_ss, nm_rs, ow_ss, ow_rs, pt_ss, pt_rs, fn_ss, fn_rs, rdy_lc, rdy_pc, rdy_b0):
+def body(n, ntp, sizes, x_hbm, wk_hbm, wv_hbm, bw_hbm, shift_hbm, dw_hbm, rate_hbm, extra_hbm, q_hbm, gate_hbm, gain_hbm, ow_hbm, st_ref, ro_ref, w_buf, x_buf, kv_buf, m_buf, t_buf, y_buf, bw_ref, shift_ref, dw_ref, rate_ref, extra_ref, q_ref, gate_ref, gain_ref, ow_ref, ab_ref, lc_in, pc_in, lc_out, pc_out, comp, rhs, rhs2, b0_in, dummy, st_in, nm_out, nm_in, ow_out, ow_all, ow_mat, part, part0, tot, fin_in, x_sem, w_sem, in_sem, lc_ss, lc_rs, pc_ss, pc_rs, b0_ss, b0_rs, st_ss, st_rs, nm_ss, nm_rs, ow_ss, ow_rs, pt_ss, pt_rs, p0_ss, p0_rs, fn_ss, fn_rs, rdy_lc, rdy_pc, rdy_b0, rdy_p0):
     grp = lax.axis_index("grp")
     z = lax.axis_index("sp")
     tp = lax.axis_index("tp")
     last = n - 1
-    prompts = ab_ref.shape[1]
+    prompts, seg, width = x_hbm.shape
     tiles = tot.shape[0]
+    span = ro_ref.shape[1]
+
+    wcopies = [
+        pltpu.make_async_copy(wk_hbm, w_buf.at[:, pl.ds(0, DK)], w_sem.at[0]),
+        pltpu.make_async_copy(wv_hbm, w_buf.at[:, pl.ds(DK, DK)], w_sem.at[1]),
+    ]
+    small = [(bw_hbm, bw_ref), (dw_hbm, dw_ref), (shift_hbm, shift_ref), (rate_hbm, rate_ref), (extra_hbm, extra_ref), (q_hbm, q_ref), (gate_hbm, gate_ref), (gain_hbm, gain_ref), (ow_hbm, ow_ref)]
+    scopies = [pltpu.make_async_copy(a, b, in_sem.at[i]) for i, (a, b) in enumerate(small)]
+    per = seg // ROWS
+    copies = []
+    for j in range(prompts * per):
+        copies.append(
+            pltpu.make_async_copy(x_hbm.at[j // per, pl.ds((j % per) * ROWS, ROWS), :], x_buf.at[pl.ds(j * ROWS, ROWS), :], x_sem.at[j])
+        )
+    for c in wcopies + scopies + copies:
+        c.start()
 
     def dev(zz, t=None):
         return (grp, zz, tp if t is None else t)
 
-    in_quad = z >= first_quad
-    pos = lax.rem(jnp.maximum(z - first_quad, 0), QUAD)
-    lc_recv = in_quad & (pos > 0)
-    lc_send = in_quad & (pos < QUAD - 1)
-    head = (z >= 1) & ((z < first_quad) | (in_quad & (pos == QUAD - 1)))
-    pc_recv = head & (z > 1)
+    ends = []
+    at = 0
+    for size in sizes:
+        at += size
+        ends.append(at)
+    starts = [e - size + 1 for e, size in zip(ends, sizes)]
+
+    def among(values):
+        hit = z == values[0]
+        for v in values[1:]:
+            hit = hit | (z == v)
+        return hit
+
+    def table(keys, values):
+        out = jnp.int32(0)
+        for k, v in zip(keys, values):
+            out = jnp.where(z == k, jnp.int32(v), out)
+        return out
+
+    head = among(ends)
+    first = among(starts)
+    lc_recv = (z >= 1) & jnp.logical_not(first)
+    lc_send = (z >= 1) & jnp.logical_not(head)
+    pc_recv = head & (z > ends[0])
     pc_send = head & (z < last)
-    prev_head = jnp.where(z <= first_quad - 1, z - 1, z - QUAD)
-    next_head = jnp.where(z < first_quad - 1, z + 1, z + QUAD)
+    prev_head = table(ends[1:], ends[:-1])
+    next_head = table(ends[:-1], ends[1:])
 
     bar = pltpu.get_barrier_semaphore()
 
     @pl.when(z == 1)
     def _():
-        for zz in range(n):
-            if zz != 1:
-                pl.semaphore_signal(bar, inc=1, device_id=dev(zz), device_id_type=MESH)
+        for zz in range(2, n):
+            pl.semaphore_signal(bar, inc=1, device_id=dev(zz), device_id_type=MESH)
         for k in range(1, ntp):
             pl.semaphore_signal(bar, inc=1, device_id=dev(z, lax.rem(tp + k, ntp)), device_id_type=MESH)
+        for k in range(ntp):
+            pl.semaphore_signal(bar, inc=1, device_id=dev(0, lax.rem(tp + k, ntp)), device_id_type=MESH)
 
     @pl.when(lc_send)
     def _():
@@ -224,11 +249,13 @@
     one = jnp.int32(1)
     zero = jnp.int32(0)
     expect = (
-        jnp.where(z == 1, ntp - 1, 1)
+        jnp.where(z == 0, ntp, jnp.where(z == 1, ntp - 1, 1))
         + jnp.where(lc_recv, one, zero)
         + jnp.where(pc_recv, one, zero)
         + jnp.where(z == last, n - 1, 0)
     )
+    scopies[8].wait()
+    ow_out[...] = ow_ref[0].astype(F32)
     pl.semaphore_wait(bar, expect)
 
     @pl.when(lc_recv)
@@ -243,7 +270,10 @@
     def _():
         pl.semaphore_signal(rdy_b0, inc=1, device_id=dev(0), device_id_type=MESH)
 
-    ow = ow_ref[0].astype(F32)
+    @pl.when(z == 0)
+    def _():
+        for k in range(ntp):
+            pl.semaphore_signal(rdy_p0, inc=1, device_id=dev(1, lax.rem(tp + k, ntp)), device_id_type=MESH)
 
     def ow_copy():
         return pltpu.make_async_remote_copy(
@@ -252,12 +282,13 @@
 
     @pl.when(z != 1)
     def _():
-        ow_out[...] = ow
         ow_copy().start()
 
     @pl.when(z == 1)
     def _():
-        ow_all[1] = ow
+        ow_all[1] = ow_out[...]
+
+    local_body(tp, prompts, seg, wcopies, copies, scopies[:8], bw_ref, dw_ref, shift_ref, rate_ref, extra_ref, ab_ref, w_buf, x_buf, kv_buf, m_buf, t_buf, y_buf)
 
     def lc_copy(src, c):
         return pltpu.make_async_remote_copy(
@@ -279,31 +310,21 @@
             a = jnp.concatenate([src[c, p] for c in range(HALF)], axis=0)
             dst[p] = right3(a)
 
-    @pl.when(lc_recv)
-    def _():
-        set_rhs(rhs, ab_ref)
+    def lc_step(c, carry):
+        lc_copy(ab_ref, c).wait_recv()
+        for p in range(prompts):
+            y = dot(left3(lc_in[c, p]), rhs[p])
+            y = y + jnp.where(c >= HALF, ab_ref[c, p], 0.0)
+            lc_out[c, p] = y
+            comp[c, p] = y
 
         @pl.when(lc_send)
         def _():
-            pl.semaphore_wait(rdy_lc, 1)
-
-        def step(c, carry):
-            lc_copy(ab_ref, c).wait_recv()
-            for p in range(prompts):
-                y = dot(left3(lc_in[c, p]), rhs[p])
-                y = y + jnp.where(c >= HALF, ab_ref[c, p], 0.0)
-                lc_out[c, p] = y
-                comp[c, p] = y
-
-            @pl.when(lc_send)
-            def _():
-                lc_copy(lc_out, c).start()
-
-            return carry
-
-        lax.fori_loop(0, NCH, step, 0)
-
-    @pl.when(lc_send & (pos == 0))
+            lc_copy(lc_out, c).start()
+
+        return carry
+
+    @pl.when(lc_send & first)
     def _():
         pl.semaphore_wait(rdy_lc, 1)
         for c in range(NCH):
@@ -321,9 +342,35 @@
         for c in range(HALF):
             b0_copy(c).start()
 
+    @pl.when(lc_recv)
+    def _():
+        set_rhs(rhs, ab_ref)
+
+        @pl.when(lc_send)
+        def _():
+            pl.semaphore_wait(rdy_lc, 1)
+
+        lax.fori_loop(0, HALF, lc_step, 0)
+
+        @pl.when(lc_send)
+        def _():
+            lax.fori_loop(HALF, NCH, lc_step, 0)
+
+    def pc_step(c, carry):
+        pc_copy(ab_ref, c).wait_recv()
+        for p in range(prompts):
+            y = dot(left3(pc_in[c, p]), rhs2[p])
+            pc_out[c, p] = y + jnp.where(c >= HALF, comp[c, p], 0.0)
+
+        @pl.when(pc_send)
+        def _():
+            pc_copy(pc_out, c).start()
+
+        return carry
+
     @pl.when(pc_recv)
     def _():
-        @pl.when(jnp.logical_not(lc_recv))
+        @pl.when(first)
         def _():
             for c in range(NCH):
                 comp[c] = ab_ref[c]
@@ -334,25 +381,31 @@
         def _():
             pl.semaphore_wait(rdy_pc, 1)
 
-        def step(c, carry):
-            pc_copy(ab_ref, c).wait_recv()
+        lax.fori_loop(0, HALF, pc_step, 0)
+
+        @pl.when(lc_recv)
+        def _():
+            lax.fori_loop(HALF, NCH, lc_step, 0)
+
+        @pl.when(z == last)
+        def _():
+            set_rhs(rhs, pc_out)
+            for c in range(HALF):
+                b0_copy(c).wait_recv()
             for p in range(prompts):
-                y = dot(left3(pc_in[c, p]), rhs2[p])
-                pc_out[c, p] = y + jnp.where(c >= HALF, comp[c, p], 0.0)
-
-            @pl.when(pc_send)
-            def _():
-                pc_copy(pc_out, c).start()
-
-            return carry
-
-        lax.fori_loop(0, NCH, step, 0)
+                start = jnp.concatenate([b0_in[c, p] for c in range(HALF)], axis=0)
+                fin = dot(left3(start), rhs[p])
+                for c in range(HALF):
+                    comp[HALF + c, p] = comp[HALF + c, p] + fin[c * CH : (c + 1) * CH]
+
+        lax.fori_loop(HALF, NCH, pc_step, 0)
+
+    tile_per = CH // 8
 
     def st_copy(zz):
         t = zz // 2
-        per = CH // 8
-        return pltpu.make_async_remote_copy(
-            src_ref=s_buf.at[t // per, :, pl.ds((t % per) * 8, 8), :], dst_ref=st_in, send_sem=st_ss.at[zz], recv_sem=st_rs, device_id=dev(zz), device_id_type=MESH
+        return pltpu.make_async_remote_copy(
+            src_ref=pc_out.at[HALF + t // tile_per, :, pl.ds((t % tile_per) * 8, 8), :], dst_ref=st_in, send_sem=st_ss.at[zz], recv_sem=st_rs, device_id=dev(zz), device_id_type=MESH
         )
 
     def nm_copy():
@@ -368,49 +421,46 @@
 
     @pl.when(z == last)
     def _():
-        set_rhs(rhs, pc_out)
-        for c in range(HALF):
-            b0_copy(c).wait_recv()
         query = q_ref[...].astype(F32)
         query = query * lax.rsqrt(jnp.sum(query * query, axis=-1, keepdims=True) + EPS) * DK**-0.5
         reads = []
         for p in range(prompts):
-            start = jnp.concatenate([b0_in[c, p] for c in range(HALF)], axis=0)
-            fin = dot(left3(start), rhs[p])
-            fin = fin + jnp.concatenate([pc_out[HALF + c, p] for c in range(HALF)], axis=0)
-            for c in range(HALF):
-                s_buf[c, p] = fin[c * CH : (c + 1) * CH]
+            fin = jnp.concatenate([pc_out[HALF + c, p] for c in range(HALF)], axis=0)
             qh, ql = split(jnp.broadcast_to(query[p : p + 1], (8, DK)))
             fh, fl = split(fin)
             read = lax.dot_general(
                 jnp.concatenate([qh, ql, qh], axis=1), jnp.concatenate([fh, fh, fl], axis=1), NT, preferred_element_type=F32
             )
             reads.append(read[0:1])
-        for zz in order:
-            st_copy(zz).start()
         read = jnp.concatenate(reads, axis=0)
         scaled = read * lax.rsqrt(jnp.mean(read * read, axis=-1, keepdims=True) + EPS)
         gate = gate_ref[...].astype(F32)
         normed = (scaled * gain_ref[...] * (gate * jax.nn.sigmoid(gate))).astype(BF16)
         nm_out[...] = normed.astype(F32)
         nm_copy().start()
+        for zz in order:
+            st_copy(zz).start()
         t = last // 2
-        per = CH // 8
         for p in range(prompts):
-            st_in[p] = s_buf[t // per, p, (t % per) * 8 : (t % per) * 8 + 8, :]
+            st_in[p] = pc_out[HALF + t // tile_per, p, (t % tile_per) * 8 : (t % tile_per) * 8 + 8, :]
 
     def pt_copy(k):
         return pltpu.make_async_remote_copy(
             src_ref=part.at[tp], dst_ref=part.at[tp], send_sem=pt_ss.at[k], recv_sem=pt_rs.at[k], device_id=dev(1, lax.rem(tp + k, ntp)), device_id_type=MESH
         )
 
+    def p0_copy(k):
+        return pltpu.make_async_remote_copy(
+            src_ref=part.at[tp, 0], dst_ref=part0.at[k], send_sem=p0_ss.at[k], recv_sem=p0_rs.at[k], device_id=dev(0, lax.rem(tp + k, ntp)), device_id_type=MESH
+        )
+
     def fin_copy(zz):
         return pltpu.make_async_remote_copy(
             src_ref=tot.at[zz // 2], dst_ref=fin_in, send_sem=fn_ss.at[zz], recv_sem=fn_rs, device_id=dev(zz), device_id_type=MESH
         )
 
-    out_order = [0] + [zz for k in range(1, n) for zz in (1 + k, (1 - k) % n) if zz < n]
-    out_order = [zz for i, zz in enumerate(out_order) if zz != 1 and zz not in out_order[:i]]
+    out_order = [zz for k in range(1, n) for zz in (1 + k, (1 - k) % n) if 1 < zz < n]
+    out_order = [zz for i, zz in enumerate(out_order) if zz not in out_order[:i]]
 
     @pl.when(z == 1)
     def _():
@@ -428,17 +478,19 @@
         half = ow_mat.shape[1] // 4
         for h in range(4):
             ow_mat[:, pl.ds(h * half, half)] = dot(perm, ow_mat[:, pl.ds(h * half, half)]).astype(BF16)
+        pl.semaphore_wait(rdy_p0, ntp)
         nm_copy().wait_recv()
         lhs = jnp.concatenate([nm_in[...], jnp.zeros((8 - prompts, DK), F32)], axis=0).astype(BF16)
-        res = dot(lhs, ow_mat[...])
-        for t in range(tiles):
-            part[tp, t] = res[0:prompts, t * 128 : (t + 1) * 128]
+        part[tp, 0] = dot(lhs, ow_mat[:, 0:128])[0:prompts]
+        for k in range(ntp):
+            p0_copy(k).start()
+        res = dot(lhs, ow_mat[:, 128:])
+        for t in range(1, tiles):
+            part[tp, t] = res[0:prompts, (t - 1) * 128 : t * 128]
         for k in range(1, ntp):
             pt_copy(k).start()
         for k in range(1, ntp):
-            pltpu.make_async_remote_copy(
-                src_ref=part.at[tp], dst_ref=part.at[tp], send_sem=pt_ss.at[k], recv_sem=pt_rs.at[k], device_id=dev(1, lax.rem(tp + k, ntp)), device_id_type=MESH
-            ).wait_recv()
+            pt_copy(k).wait_recv()
         acc = part[0]
         for k in range(1, ntp):
             acc = acc + part[k]
@@ -457,21 +509,29 @@
     for p in range(prompts):
         st_ref[p] = jnp.where(odd == 1, st_in[p, 4:8, :], st_in[p, 0:4, :]).astype(BF16)
 
-    @pl.when(z != 1)
+    @pl.when(z > 1)
     def _():
         pltpu.make_async_remote_copy(
             src_ref=fin_in, dst_ref=fin_in, send_sem=fn_ss.at[0], recv_sem=fn_rs, device_id=dev(1), device_id_type=MESH
         ).wait_recv()
 
-    span = ro_ref.shape[1]
-    first = odd * (ntp * span) + tp * span
+    @pl.when(z == 0)
+    def _():
+        for k in range(ntp):
+            p0_copy(k).wait_recv()
+        acc = part0[0]
+        for k in range(1, ntp):
+            acc = acc + part0[k]
+        fin_in[...] = acc
+
+    at = odd * (ntp * span) + tp * span
     value = fin_in[...]
     lane = lax.broadcasted_iota(jnp.int32, (128, span), 0)
-    want = lax.broadcasted_iota(jnp.int32, (128, span), 1) + first
+    want = lax.broadcasted_iota(jnp.int32, (128, span), 1) + at
     v1, v2 = split(value)
     v3 = (value - v1.astype(F32) - v2.astype(F32)).astype(BF16)
     sel = jnp.where(lane == want, 1.0, 0.0).astype(BF16)
-    ro_ref[...] = dot(v1, sel) + dot(v2, sel) + dot(v3, sel)
+    ro_ref[...] = dot(jnp.concatenate([v1, v2, v3], axis=1), jnp.concatenate([sel, sel, sel], axis=0))
 
     @pl.when(z != 1)
     def _():
@@ -503,85 +563,93 @@
     def _():
         for k in range(1, ntp):
             pt_copy(k).wait_send()
-        for zz in range(n):
-            if zz != 1:
-                fin_copy(zz).wait_send()
+        for k in range(ntp):
+            p0_copy(k).wait_send()
+        for zz in range(2, n):
+            fin_copy(zz).wait_send()
 
 
 VM = pl.BlockSpec(memory_space=pltpu.VMEM)
-SM = pl.BlockSpec(memory_space=pltpu.SMEM)
 ANY = pl.BlockSpec(memory_space=pl.ANY)
 
 
-def local_map(x, wk, wv, bw, dw, shift, rate, extra):
+def fused(n, ntp, x, wk, wv, bw, shift, dw, rate, extra, q, gate, gain, ow):
     prompts, seg, width = x.shape
     total = prompts * seg
     groups = total // BLK
-    chunks = total // 256
+    chunks = total // ROWS
+    lines = ow.shape[1]
+    sizes = GROUPS if n == sum(GROUPS) + 1 else (1,) * (n - 1)
+    span = ow.shape[2] // (n * ntp)
+    tiles = ow.shape[2] // 128
+    vm = pltpu.VMEM
+    blk = vm((NCH, prompts, CH, DK), F32)
+    dma = pltpu.SemaphoreType.DMA
+    reg = pltpu.SemaphoreType.REGULAR
+    square = vm((groups, BLK, BLK), F32)
+    small = [vm(a.shape, a.dtype) for a in (bw, shift, dw, rate, extra, q, gate, gain, ow)]
     return pl.pallas_call(
-        local_body,
-        name="local_map",
-        out_shape=jax.ShapeDtypeStruct((NCH, prompts, CH, DK), F32),
-        in_specs=[ANY, ANY, ANY, VM, VM, SM, SM, VM],
-        out_specs=VM,
-        scratch_shapes=[
-            pltpu.VMEM((width, 2 * DK), BF16),
-            pltpu.VMEM((total, width), BF16),
-            pltpu.VMEM((total, 2 * DK), BF16),
-            pltpu.VMEM((groups, BLK, BLK), F32),
-            pltpu.VMEM((groups, BLK, BLK), F32),
-            pltpu.VMEM((groups, BLK, BLK), F32),
-            pltpu.SemaphoreType.DMA((chunks,)),
-            pltpu.SemaphoreType.DMA((2,)),
-        ],
-    )(x, wk, wv, bw, dw, shift, rate, extra)
-
-
-def exchange(n, ntp, ab, q, gate, gain, ow):
-    prompts = ab.shape[1]
-    width = ow.shape[2]
-    lines = ow.shape[1]
-    quads = 3 if n >= 32 else 1
-    first_quad = n - QUAD * quads
-    span = width // (n * ntp)
-    tiles = width // 128
-    blk = pltpu.VMEM((NCH, prompts, CH, DK), F32)
-    dma = pltpu.SemaphoreType.DMA
-    return pl.pallas_call(
-        functools.partial(comm_body, n, ntp, first_quad),
-        name="exchange",
+        functools.partial(body, n, ntp, sizes),
+        name="delta_states",
         out_shape=(
             jax.ShapeDtypeStruct((prompts, lines, DK), BF16),
             jax.ShapeDtypeStruct((prompts, span), F32),
         ),
-        in_specs=[VM] * 5,
+        in_specs=[ANY] * 12,
         out_specs=(VM, VM),
         scratch_shapes=[
-            blk, blk, blk, blk, blk,
-            pltpu.VMEM((prompts, 3 * DK, DK), BF16),
-            pltpu.VMEM((prompts, 3 * DK, DK), BF16),
-            pltpu.VMEM((HALF, prompts, CH, DK), F32),
-            pltpu.VMEM((HALF, prompts, CH, DK), F32),
-            pltpu.VMEM((prompts, 8, DK), F32),
-            pltpu.VMEM((prompts, DK), F32),
-            pltpu.VMEM((prompts, DK), F32),
-            pltpu.VMEM((lines, width), F32),
-            pltpu.VMEM((n, lines, width), F32),
-            pltpu.VMEM((n * lines, width), BF16),
-            pltpu.VMEM((ntp, tiles, prompts, 128), F32),
-            pltpu.VMEM((tiles, prompts, 128), F32),
-            pltpu.VMEM((prompts, 128), F32),
+            vm((width, 2 * DK), BF16),
+            vm((total, width), BF16),
+            vm((total, 2 * DK), BF16),
+            square, square, square,
+            *small,
+            blk, blk, blk, blk, blk, blk,
+            vm((prompts, 3 * DK, DK), BF16),
+            vm((prompts, 3 * DK, DK), BF16),
+            vm((HALF, prompts, CH, DK), F32),
+            vm((prompts, 8, DK), F32),
+            vm((prompts, 8, DK), F32),
+            vm((prompts, DK), F32),
+            vm((prompts, DK), F32),
+            vm((lines, ow.shape[2]), F32),
+            vm((n, lines, ow.shape[2]), F32),
+            vm((n * lines, ow.shape[2]), BF16),
+            vm((ntp, tiles, prompts, 128), F32),
+            vm((ntp, prompts, 128), F32),
+            vm((tiles, prompts, 128), F32),
+            vm((prompts, 128), F32),
+            dma((chunks,)), dma((2,)), dma((9,)),
             dma((NCH,)), dma((NCH,)), dma((NCH,)), dma((NCH,)),
             dma((HALF,)), dma((HALF,)),
             dma((n,)), dma,
             dma, dma,
             dma, dma((n,)),
             dma((ntp,)), dma((ntp,)),
+            dma((ntp,)), dma((ntp,)),
             dma((n,)), dma,
-            pltpu.SemaphoreType.REGULAR, pltpu.SemaphoreType.REGULAR, pltpu.SemaphoreType.REGULAR,
+            reg, reg, reg, reg,
         ],
         compiler_params=pltpu.CompilerParams(collective_id=0, has_side_effects=True),
-    )(ab, q, gate, gain, ow)
+    )(x, wk, wv, bw, shift, dw, rate, extra, q, gate, gain, ow)
+
+
+def hand_over(st_in, ro_in, st_out, ro_out, sem):
+    copies = [pltpu.make_async_copy(st_in, st_out, sem.at[0]), pltpu.make_async_copy(ro_in, ro_out, sem.at[1])]
+    for c in copies:
+        c.start()
+    for c in copies:
+        c.wait()
+
+
+def finish(st, ro):
+    return pl.pallas_call(
+        hand_over,
+        name="hand_over",
+        out_shape=(jax.ShapeDtypeStruct(st.shape, st.dtype), jax.ShapeDtypeStruct(ro.shape, ro.dtype)),
+        in_specs=[ANY, ANY],
+        out_specs=(ANY, ANY),
+        scratch_shapes=[pltpu.SemaphoreType.DMA((2,))],
+    )(st, ro)
 
 
 def solution(mesh):
@@ -589,8 +657,8 @@
 
     def per_device(x, wk, wv, bw, shift, dw, rate, extra, q, gate, gain, ow):
         prompts, seg, width = x.shape
-        ab = local_map(x, wk, wv, bw.T, dw.T, shift, rate, extra.reshape(prompts, 1, seg))
-        st, ro = exchange(n, ntp, ab, q, gate, gain.reshape(1, -1), ow)
+        st, ro = fused(n, ntp, x, wk, wv, bw.T, shift.reshape(1, -1), dw.T, rate.reshape(1, -1), extra.reshape(prompts, 1, seg), q, gate, gain.reshape(1, -1), ow)
+        st, ro = finish(st, ro)
         return jnp.transpose(st, (0, 2, 1))[:, None], ro
 
     placed = (

time: 114 us -> 91.1 us (0.80)
  Pallas kernels: 110 us -> 89.3 us
  local copies, waits for them, and re-layouts: 2.48 us -> 0 us
    pallas_call x2, Pallas kernels: 110 us -> 89.3 us  [the longest x1 88.1 us: fused(): pl.pallas_call(functools.partial(body, n, ntp, sizes), name='delta_states...]
    unnamed x2 -> x0, local copies, waits for them, and re-layouts: 2.48 us -> none
where the time goes in v2:
time: 91.1 us; the launch traced here: 89.9 us
  Pallas kernels  89.3 us (98%)
    pallas_call x1, Pallas kernels, fused(): pl.pallas_call(functools.partial(body, n, ntp, sizes), name='delta_states...  88.1 us

profile of v2, /device:TPU:40, one launch (start us, length us, event | category | flops | bytes accessed | tf_op | source)
XLA Modules:
  0.0 89.9 jit_solution(4284168090340602230)
XLA Ops:
  0.6 88.1 %delta_states.1 = (bf16[2,4,128]{2,1,0:T(4,128)(2,1)}, f32[2,8]{1,0:T(2,128)}) custom-call(bf16[2,512,2048]{2,1,0:T(8,128)(2,1)} %x_hbm.1, bf16[2048,128]{1,0:T(8,128)(2,1)} %wk_hbm.1, bf16[2048,128]{1,0:T(8,128)(2,1)} %wv_hbm.1, bf16[8,2048]{1,0:T(8,128)(2,1)} %bitcast.11, f32[1,8]{1,0:T(1,128)} %bitcast.14, bf16[8,2048]{1,0:T(8,128)(2,1)} %bitcast.12, ...), custom_call_target="tpu_custom_call" | custom-call | tf_op jit(solution)/shard_map/delta_states/pallas_call | solution.py:591
  88.7 1.2 %hand_over.1 = (bf16[2,4,128]{2,1,0:T(4,128)(2,1)}, f32[2,8]{1,0:T(2,128)}) custom-call(bf16[2,4,128]{2,1,0:T(4,128)(2,1)} %get-tuple-element.6.st_in, f32[2,8]{1,0:T(2,128)} %get-tuple-element.7.ro_in), custom_call_target="tpu_custom_call" | custom-call | tf_op jit(solution)/shard_map/hand_over/pallas_call | solution.py:645

commit v3 on v2

--- a/solution.py
+++ b/solution.py
@@ -17,7 +17,7 @@
 ROWS = 256
 HALF = DK // CH
 NCH = 2 * HALF
-GROUPS = (1, 1, 1, 1, 1, 2, 2, 2, 2, 2, 3, 3, 4, 6)
+GROUPS = (1, 1, 1, 1, 1, 2, 2, 2, 2, 2, 3, 4, 4, 5)
 NT = (((1,), (1,)), ((), ()))
 
 
@@ -48,20 +48,23 @@
     return dot(left3(a), right3(b))
 
 
-def local_body(tp, prompts, seg, wcopies, copies, scopies, bw_ref, dw_ref, shift_ref, rate_ref, extra_ref, ab_ref, w_buf, x_buf, kv_buf, m_buf, t_buf, y_buf):
+def local_body(middle, tp, prompts, seg, wcopies, copies, scopies, bw_ref, dw_ref, shift_ref, rate_ref, extra_ref, ab_ref, w_buf, x_buf, kv_buf, m_buf, t_buf, y_buf):
     rows = ROWS
     chunks = len(copies)
-    for c in scopies:
-        c.wait()
-    wbd = jnp.concatenate([bw_ref[...], dw_ref[...]], axis=0)
     for c in wcopies:
         c.wait()
+    for c in copies[1:]:
+        c.start()
+    wbd = jnp.concatenate([bw_ref[...], dw_ref[...]], axis=0)
     raw = []
     for j in range(chunks):
         copies[j].wait()
         xs = x_buf[pl.ds(j * rows, rows), :]
         kv_buf[pl.ds(j * rows, rows), :] = dot(xs, w_buf[...]).astype(BF16)
         raw.append(lax.dot_general(wbd, xs, NT, preferred_element_type=F32))
+    middle()
+    for c in scopies:
+        c.wait()
     groups = prompts * seg // BLK
     gp = seg // BLK
     heads = bw_ref.shape[0]
@@ -168,7 +171,7 @@
                 ab_ref[c, p] = maps[0][c * CH : (c + 1) * CH]
 
 
-def body(n, ntp, sizes, x_hbm, wk_hbm, wv_hbm, bw_hbm, shift_hbm, dw_hbm, rate_hbm, extra_hbm, q_hbm, gate_hbm, gain_hbm, ow_hbm, st_ref, ro_ref, w_buf, x_buf, kv_buf, m_buf, t_buf, y_buf, bw_ref, shift_ref, dw_ref, rate_ref, extra_ref, q_ref, gate_ref, gain_ref, ow_ref, ab_ref, lc_in, pc_in, lc_out, pc_out, comp, rhs, rhs2, b0_in, dummy, st_in, nm_out, nm_in, ow_out, ow_all, ow_mat, part, part0, tot, fin_in, x_sem, w_sem, in_sem, lc_ss, lc_rs, pc_ss, pc_rs, b0_ss, b0_rs, st_ss, st_rs, nm_ss, nm_rs, ow_ss, ow_rs, pt_ss, pt_rs, p0_ss, p0_rs, fn_ss, fn_rs, rdy_lc, rdy_pc, rdy_b0, rdy_p0):
+def body(n, ntp, sizes, x_hbm, wk_hbm, wv_hbm, bw_hbm, shift_hbm, dw_hbm, rate_hbm, extra_hbm, q_hbm, gate_hbm, gain_hbm, ow_hbm, st_ref, ro_ref, w_buf, x_buf, kv_buf, m_buf, t_buf, y_buf, bw_ref, shift_ref, dw_ref, rate_ref, extra_ref, q_ref, gate_ref, gain_ref, ow_ref, ab_ref, lc_in, pc_in, lc_out, pc_out, comp, rhs, rhs2, b0_in, dummy, st_in, nm_out, nm_in, ow_out, ow_all, ow_mat, part, part0, tot, fin_in, st_size, fn_size, x_sem, w_sem, in_sem, lc_ss, lc_rs, pc_ss, pc_rs, b0_ss, b0_rs, st_ss, st_rs, nm_ss, nm_rs, ow_ss, ow_rs, pt_ss, pt_rs, p0_ss, p0_rs, fn_ss, fn_rs, rdy_lc, rdy_pc, rdy_b0, rdy_p0):
     grp = lax.axis_index("grp")
     z = lax.axis_index("sp")
     tp = lax.axis_index("tp")
@@ -181,7 +184,8 @@
         pltpu.make_async_copy(wk_hbm, w_buf.at[:, pl.ds(0, DK)], w_sem.at[0]),
         pltpu.make_async_copy(wv_hbm, w_buf.at[:, pl.ds(DK, DK)], w_sem.at[1]),
     ]
-    small = [(bw_hbm, bw_ref), (dw_hbm, dw_ref), (shift_hbm, shift_ref), (rate_hbm, rate_ref), (extra_hbm, extra_ref), (q_hbm, q_ref), (gate_hbm, gate_ref), (gain_hbm, gain_ref), (ow_hbm, ow_ref)]
+    wcopies += [pltpu.make_async_copy(bw_hbm, bw_ref, w_sem.at[2]), pltpu.make_async_copy(dw_hbm, dw_ref, w_sem.at[3])]
+    small = [(shift_hbm, shift_ref), (rate_hbm, rate_ref), (extra_hbm, extra_ref), (q_hbm, q_ref), (gate_hbm, gate_ref), (gain_hbm, gain_ref), (ow_hbm, ow_ref)]
     scopies = [pltpu.make_async_copy(a, b, in_sem.at[i]) for i, (a, b) in enumerate(small)]
     per = seg // ROWS
     copies = []
@@ -189,7 +193,7 @@
         copies.append(
             pltpu.make_async_copy(x_hbm.at[j // per, pl.ds((j % per) * ROWS, ROWS), :], x_buf.at[pl.ds(j * ROWS, ROWS), :], x_sem.at[j])
         )
-    for c in wcopies + scopies + copies:
+    for c in wcopies:
         c.start()
 
     def dev(zz, t=None):
@@ -246,6 +250,9 @@
     def _():
         pl.semaphore_signal(bar, inc=1, device_id=dev(last), device_id_type=MESH)
 
+    copies[0].start()
+    for c in scopies:
+        c.start()
     one = jnp.int32(1)
     zero = jnp.int32(0)
     expect = (
@@ -254,55 +261,56 @@
         + jnp.where(pc_recv, one, zero)
         + jnp.where(z == last, n - 1, 0)
     )
-    scopies[8].wait()
-    ow_out[...] = ow_ref[0].astype(F32)
-    pl.semaphore_wait(bar, expect)
-
-    @pl.when(lc_recv)
-    def _():
-        pl.semaphore_signal(rdy_lc, inc=1, device_id=dev(z - 1), device_id_type=MESH)
-
-    @pl.when(pc_recv)
-    def _():
-        pl.semaphore_signal(rdy_pc, inc=1, device_id=dev(prev_head), device_id_type=MESH)
-
-    @pl.when(z == last)
-    def _():
-        pl.semaphore_signal(rdy_b0, inc=1, device_id=dev(0), device_id_type=MESH)
-
-    @pl.when(z == 0)
-    def _():
-        for k in range(ntp):
-            pl.semaphore_signal(rdy_p0, inc=1, device_id=dev(1, lax.rem(tp + k, ntp)), device_id_type=MESH)
-
     def ow_copy():
         return pltpu.make_async_remote_copy(
-            src_ref=ow_out, dst_ref=ow_all.at[z], send_sem=ow_ss, recv_sem=ow_rs.at[z], device_id=dev(1), device_id_type=MESH
-        )
-
-    @pl.when(z != 1)
-    def _():
-        ow_copy().start()
-
-    @pl.when(z == 1)
-    def _():
-        ow_all[1] = ow_out[...]
-
-    local_body(tp, prompts, seg, wcopies, copies, scopies[:8], bw_ref, dw_ref, shift_ref, rate_ref, extra_ref, ab_ref, w_buf, x_buf, kv_buf, m_buf, t_buf, y_buf)
+            src_ref=ow_out, dst_ref=ow_all.at[z], send_sem=ow_ss, recv_sem=ow_rs, device_id=dev(1), device_id_type=MESH
+        )
+
+    def middle():
+        scopies[6].wait()
+        ow_out[...] = ow_ref[0].astype(F32)
+        pl.semaphore_wait(bar, expect)
+
+        @pl.when(lc_recv)
+        def _():
+            pl.semaphore_signal(rdy_lc, inc=1, device_id=dev(z - 1), device_id_type=MESH)
+
+        @pl.when(pc_recv)
+        def _():
+            pl.semaphore_signal(rdy_pc, inc=1, device_id=dev(prev_head), device_id_type=MESH)
+
+        @pl.when(z == last)
+        def _():
+            pl.semaphore_signal(rdy_b0, inc=1, device_id=dev(0), device_id_type=MESH)
+
+        @pl.when(z == 0)
+        def _():
+            for k in range(ntp):
+                pl.semaphore_signal(rdy_p0, inc=1, device_id=dev(1, lax.rem(tp + k, ntp)), device_id_type=MESH)
+
+        @pl.when(z != 1)
+        def _():
+            ow_copy().start()
+
+        @pl.when(z == 1)
+        def _():
+            ow_all[1] = ow_out[...]
+
+    local_body(middle, tp, prompts, seg, wcopies, copies, scopies[:6], bw_ref, dw_ref, shift_ref, rate_ref, extra_ref, ab_ref, w_buf, x_buf, kv_buf, m_buf, t_buf, y_buf)
 
     def lc_copy(src, c):
         return pltpu.make_async_remote_copy(
-            src_ref=src.at[c], dst_ref=lc_in.at[c], send_sem=lc_ss.at[c], recv_sem=lc_rs.at[c], device_id=dev(z + 1), device_id_type=MESH
+            src_ref=src.at[c], dst_ref=lc_in.at[c], send_sem=lc_ss, recv_sem=lc_rs.at[c], device_id=dev(z + 1), device_id_type=MESH
         )
 
     def pc_copy(src, c):
         return pltpu.make_async_remote_copy(
-            src_ref=src.at[c], dst_ref=pc_in.at[c], send_sem=pc_ss.at[c], recv_sem=pc_rs.at[c], device_id=dev(next_head), device_id_type=MESH
-        )
-
-    def b0_copy(c):
-        return pltpu.make_async_remote_copy(
-            src_ref=ab_ref.at[HALF + c], dst_ref=b0_in.at[c], send_sem=b0_ss.at[c], recv_sem=b0_rs.at[c], device_id=dev(last), device_id_type=MESH
+            src_ref=src.at[c], dst_ref=pc_in.at[c], send_sem=pc_ss, recv_sem=pc_rs.at[c], device_id=dev(next_head), device_id_type=MESH
+        )
+
+    def b0_copy():
+        return pltpu.make_async_remote_copy(
+            src_ref=ab_ref.at[pl.ds(HALF, HALF)], dst_ref=b0_in, send_sem=b0_ss, recv_sem=b0_rs, device_id=dev(last), device_id_type=MESH
         )
 
     def set_rhs(dst, src):
@@ -339,8 +347,7 @@
     @pl.when(z == 0)
     def _():
         pl.semaphore_wait(rdy_b0, 1)
-        for c in range(HALF):
-            b0_copy(c).start()
+        b0_copy().start()
 
     @pl.when(lc_recv)
     def _():
@@ -352,7 +359,7 @@
 
         lax.fori_loop(0, HALF, lc_step, 0)
 
-        @pl.when(lc_send)
+        @pl.when(lc_send | (z == last))
         def _():
             lax.fori_loop(HALF, NCH, lc_step, 0)
 
@@ -383,15 +390,14 @@
 
         lax.fori_loop(0, HALF, pc_step, 0)
 
-        @pl.when(lc_recv)
+        @pl.when(lc_recv & (z != last))
         def _():
             lax.fori_loop(HALF, NCH, lc_step, 0)
 
         @pl.when(z == last)
         def _():
             set_rhs(rhs, pc_out)
-            for c in range(HALF):
-                b0_copy(c).wait_recv()
+            b0_copy().wait_recv()
             for p in range(prompts):
                 start = jnp.concatenate([b0_in[c, p] for c in range(HALF)], axis=0)
                 fin = dot(left3(start), rhs[p])
@@ -405,7 +411,7 @@
     def st_copy(zz):
         t = zz // 2
         return pltpu.make_async_remote_copy(
-            src_ref=pc_out.at[HALF + t // tile_per, :, pl.ds((t % tile_per) * 8, 8), :], dst_ref=st_in, send_sem=st_ss.at[zz], recv_sem=st_rs, device_id=dev(zz), device_id_type=MESH
+            src_ref=pc_out.at[HALF + t // tile_per, :, pl.ds((t % tile_per) * 8, 8), :], dst_ref=st_in, send_sem=st_ss, recv_sem=st_rs, device_id=dev(zz), device_id_type=MESH
         )
 
     def nm_copy():
@@ -446,17 +452,28 @@
 
     def pt_copy(k):
         return pltpu.make_async_remote_copy(
-            src_ref=part.at[tp], dst_ref=part.at[tp], send_sem=pt_ss.at[k], recv_sem=pt_rs.at[k], device_id=dev(1, lax.rem(tp + k, ntp)), device_id_type=MESH
+            src_ref=part.at[tp], dst_ref=part.at[tp], send_sem=pt_ss, recv_sem=pt_rs, device_id=dev(1, lax.rem(tp + k, ntp)), device_id_type=MESH
+        )
+
+    def pt_all():
+        some = part.at[pl.ds(0, ntp - 1)]
+        return pltpu.make_async_remote_copy(
+            src_ref=some, dst_ref=some, send_sem=pt_ss, recv_sem=pt_rs, device_id=dev(0), device_id_type=MESH
+        )
+
+    def p0_all():
+        return pltpu.make_async_remote_copy(
+            src_ref=part0, dst_ref=part0, send_sem=p0_ss, recv_sem=p0_rs, device_id=dev(last), device_id_type=MESH
         )
 
     def p0_copy(k):
         return pltpu.make_async_remote_copy(
-            src_ref=part.at[tp, 0], dst_ref=part0.at[k], send_sem=p0_ss.at[k], recv_sem=p0_rs.at[k], device_id=dev(0, lax.rem(tp + k, ntp)), device_id_type=MESH
+            src_ref=part.at[tp, 0], dst_ref=part0.at[tp], send_sem=p0_ss, recv_sem=p0_rs, device_id=dev(0, lax.rem(tp + k, ntp)), device_id_type=MESH
         )
 
     def fin_copy(zz):
         return pltpu.make_async_remote_copy(
-            src_ref=tot.at[zz // 2], dst_ref=fin_in, send_sem=fn_ss.at[zz], recv_sem=fn_rs, device_id=dev(zz), device_id_type=MESH
+            src_ref=tot.at[zz // 2], dst_ref=fin_in, send_sem=fn_ss, recv_sem=fn_rs, device_id=dev(zz), device_id_type=MESH
         )
 
     out_order = [zz for k in range(1, n) for zz in (1 + k, (1 - k) % n) if 1 < zz < n]
@@ -464,11 +481,9 @@
 
     @pl.when(z == 1)
     def _():
-        for zz in range(n):
-            if zz != 1:
-                pltpu.make_async_remote_copy(
-                    src_ref=ow_out, dst_ref=ow_all.at[zz], send_sem=ow_ss, recv_sem=ow_rs.at[zz], device_id=dev(1), device_id_type=MESH
-                ).wait_recv()
+        pltpu.make_async_remote_copy(
+            src_ref=ow_all.at[pl.ds(0, n - 1)], dst_ref=ow_all.at[pl.ds(0, n - 1)], send_sem=ow_ss, recv_sem=ow_rs, device_id=dev(0), device_id_type=MESH
+        ).wait_recv()
         lines = ow_all.shape[1]
         for r in range(lines):
             ow_mat[pl.ds(r * n, n), :] = ow_all[:, r, :].astype(BF16)
@@ -489,8 +504,7 @@
             part[tp, t] = res[0:prompts, (t - 1) * 128 : t * 128]
         for k in range(1, ntp):
             pt_copy(k).start()
-        for k in range(1, ntp):
-            pt_copy(k).wait_recv()
+        pt_all().wait_recv()
         acc = part[0]
         for k in range(1, ntp):
             acc = acc + part[k]
@@ -502,7 +516,7 @@
     @pl.when(z != last)
     def _():
         pltpu.make_async_remote_copy(
-            src_ref=st_in, dst_ref=st_in, send_sem=st_ss.at[0], recv_sem=st_rs, device_id=dev(last), device_id_type=MESH
+            src_ref=st_in, dst_ref=st_in, send_sem=st_ss, recv_sem=st_rs, device_id=dev(last), device_id_type=MESH
         ).wait_recv()
 
     odd = lax.rem(z, 2)
@@ -512,13 +526,12 @@
     @pl.when(z > 1)
     def _():
         pltpu.make_async_remote_copy(
-            src_ref=fin_in, dst_ref=fin_in, send_sem=fn_ss.at[0], recv_sem=fn_rs, device_id=dev(1), device_id_type=MESH
+            src_ref=fin_in, dst_ref=fin_in, send_sem=fn_ss, recv_sem=fn_rs, device_id=dev(1), device_id_type=MESH
         ).wait_recv()
 
     @pl.when(z == 0)
     def _():
-        for k in range(ntp):
-            p0_copy(k).wait_recv()
+        p0_all().wait_recv()
         acc = part0[0]
         for k in range(1, ntp):
             acc = acc + part0[k]
@@ -539,34 +552,34 @@
 
     @pl.when(lc_send)
     def _():
-        for c in range(NCH):
-            lc_copy(lc_out, c).wait_send()
+        pltpu.make_async_remote_copy(
+            src_ref=lc_out, dst_ref=lc_in, send_sem=lc_ss, recv_sem=lc_rs.at[0], device_id=dev(z + 1), device_id_type=MESH
+        ).wait_send()
 
     @pl.when(pc_send)
     def _():
-        for c in range(NCH):
-            pc_copy(pc_out, c).wait_send()
+        pltpu.make_async_remote_copy(
+            src_ref=pc_out, dst_ref=pc_in, send_sem=pc_ss, recv_sem=pc_rs.at[0], device_id=dev(next_head), device_id_type=MESH
+        ).wait_send()
 
     @pl.when(z == 0)
     def _():
-        for c in range(HALF):
-            b0_copy(c).wait_send()
+        b0_copy().wait_send()
 
     @pl.when(z == last)
     def _():
-        for zz in range(n):
-            if zz != last:
-                st_copy(zz).wait_send()
+        pltpu.make_async_remote_copy(
+            src_ref=st_size, dst_ref=st_size, send_sem=st_ss, recv_sem=st_rs, device_id=dev(0), device_id_type=MESH
+        ).wait_send()
         nm_copy().wait_send()
 
     @pl.when(z == 1)
     def _():
-        for k in range(1, ntp):
-            pt_copy(k).wait_send()
-        for k in range(ntp):
-            p0_copy(k).wait_send()
-        for zz in range(2, n):
-            fin_copy(zz).wait_send()
+        pt_all().wait_send()
+        p0_all().wait_send()
+        pltpu.make_async_remote_copy(
+            src_ref=fn_size, dst_ref=fn_size, send_sem=fn_ss, recv_sem=fn_rs, device_id=dev(0), device_id_type=MESH
+        ).wait_send()
 
 
 VM = pl.BlockSpec(memory_space=pltpu.VMEM)
@@ -592,8 +605,8 @@
         functools.partial(body, n, ntp, sizes),
         name="delta_states",
         out_shape=(
-            jax.ShapeDtypeStruct((prompts, lines, DK), BF16),
-            jax.ShapeDtypeStruct((prompts, span), F32),
+            pltpu.VMEM((prompts, lines, DK), BF16),
+            pltpu.VMEM((prompts, span), F32),
         ),
         in_specs=[ANY] * 12,
         out_specs=(VM, VM),
@@ -618,15 +631,17 @@
             vm((ntp, prompts, 128), F32),
             vm((tiles, prompts, 128), F32),
             vm((prompts, 128), F32),
-            dma((chunks,)), dma((2,)), dma((9,)),
-            dma((NCH,)), dma((NCH,)), dma((NCH,)), dma((NCH,)),
-            dma((HALF,)), dma((HALF,)),
-            dma((n,)), dma,
+            vm((n - 1, prompts, 8, DK), F32),
+            vm((n - 2, prompts, 128), F32),
+            dma((chunks,)), dma((4,)), dma((7,)),
+            dma, dma((NCH,)), dma, dma((NCH,)),
             dma, dma,
-            dma, dma((n,)),
-            dma((ntp,)), dma((ntp,)),
-            dma((ntp,)), dma((ntp,)),
-            dma((n,)), dma,
+            dma, dma,
+            dma, dma,
+            dma, dma,
+            dma, dma,
+            dma, dma,
+            dma, dma,
             reg, reg, reg, reg,
         ],
         compiler_params=pltpu.CompilerParams(collective_id=0, has_side_effects=True),
@@ -649,6 +664,7 @@
         in_specs=[ANY, ANY],
         out_specs=(ANY, ANY),
         scratch_shapes=[pltpu.SemaphoreType.DMA((2,))],
+        compiler_params=pltpu.CompilerParams(vmem_limit_bytes=1024 * 1024),
     )(st, ro)
 
 

time: 91.1 us -> 86.2 us (0.946)
  Pallas kernels: 89.3 us -> 84.4 us
    pallas_call x1, Pallas kernels: 88.1 us -> 83.8 us  [fused(): pl.pallas_call(functools.partial(body, n, ntp, sizes), name='delta_states...]
where the time goes in v3:
time: 86.2 us; the launch traced here: 85 us
  Pallas kernels  84.4 us (98%)
    pallas_call x1, Pallas kernels, fused(): pl.pallas_call(functools.partial(body, n, ntp, sizes), name='delta_states...  83.8 us

profile of v3, /device:TPU:40, one launch (start us, length us, event | category | flops | bytes accessed | tf_op | source)
XLA Modules:
  0.0 85.0 jit_solution(15773980180200035169)
XLA Ops:
  0.6 83.8 %delta_states.1 = (bf16[2,4,128]{2,1,0:T(4,128)(2,1)S(1)}, f32[2,8]{1,0:T(2,128)S(1)}) custom-call(bf16[2,512,2048]{2,1,0:T(8,128)(2,1)} %x_hbm.1, bf16[2048,128]{1,0:T(8,128)(2,1)} %wk_hbm.1, bf16[2048,128]{1,0:T(8,128)(2,1)} %wv_hbm.1, bf16[8,2048]{1,0:T(8,128)(2,1)} %bitcast.11, f32[1,8]{1,0:T(1,128)} %bitcast.14, bf16[8,2048]{1,0:T(8,128)(2,1)} %bitcast.12, ...), custom_call_target="tpu_custom_call" | custom-call | tf_op jit(solution)/shard_map/delta_states/pallas_call | solution.py:604
  84.4 0.6 hand_over.1

commit v4 on v3

--- a/solution.py
+++ b/solution.py
@@ -222,10 +222,13 @@
     first = among(starts)
     lc_recv = (z >= 1) & jnp.logical_not(first)
     lc_send = (z >= 1) & jnp.logical_not(head)
-    pc_recv = head & (z > ends[0])
-    pc_send = head & (z < last)
+    carry = tp == 0
+    late = (z == 0) & carry
+    opens = (z == 0) & jnp.logical_not(carry)
+    pc_recv = head & ((z > ends[0]) | jnp.logical_not(carry))
+    pc_send = (head & (z < last)) | opens
     prev_head = table(ends[1:], ends[:-1])
-    next_head = table(ends[:-1], ends[1:])
+    next_head = jnp.where(z == 0, ends[0], table(ends[:-1], ends[1:]))
 
     bar = pltpu.get_barrier_semaphore()
 
@@ -279,7 +282,7 @@
         def _():
             pl.semaphore_signal(rdy_pc, inc=1, device_id=dev(prev_head), device_id_type=MESH)
 
-        @pl.when(z == last)
+        @pl.when((z == last) & carry)
         def _():
             pl.semaphore_signal(rdy_b0, inc=1, device_id=dev(0), device_id_type=MESH)
 
@@ -338,13 +341,19 @@
         for c in range(NCH):
             lc_copy(ab_ref, c).start()
 
-    @pl.when((z == 1) & pc_send)
+    @pl.when((z == ends[0]) & carry)
     def _():
         pl.semaphore_wait(rdy_pc, 1)
         for c in range(NCH):
             pc_copy(ab_ref, c).start()
 
-    @pl.when(z == 0)
+    @pl.when(opens)
+    def _():
+        pl.semaphore_wait(rdy_pc, 1)
+        for c in range(HALF, NCH):
+            pc_copy(ab_ref, c).start()
+
+    @pl.when(late)
     def _():
         pl.semaphore_wait(rdy_b0, 1)
         b0_copy().start()
@@ -388,13 +397,15 @@
         def _():
             pl.semaphore_wait(rdy_pc, 1)
 
-        lax.fori_loop(0, HALF, pc_step, 0)
+        @pl.when(carry)
+        def _():
+            lax.fori_loop(0, HALF, pc_step, 0)
 
         @pl.when(lc_recv & (z != last))
         def _():
             lax.fori_loop(HALF, NCH, lc_step, 0)
 
-        @pl.when(z == last)
+        @pl.when((z == last) & carry)
         def _():
             set_rhs(rhs, pc_out)
             b0_copy().wait_recv()
@@ -556,13 +567,20 @@
             src_ref=lc_out, dst_ref=lc_in, send_sem=lc_ss, recv_sem=lc_rs.at[0], device_id=dev(z + 1), device_id_type=MESH
         ).wait_send()
 
-    @pl.when(pc_send)
-    def _():
+    def pc_sent(rows):
         pltpu.make_async_remote_copy(
-            src_ref=pc_out, dst_ref=pc_in, send_sem=pc_ss, recv_sem=pc_rs.at[0], device_id=dev(next_head), device_id_type=MESH
+            src_ref=pc_out.at[rows], dst_ref=pc_in.at[rows], send_sem=pc_ss, recv_sem=pc_rs.at[0], device_id=dev(next_head), device_id_type=MESH
         ).wait_send()
 
-    @pl.when(z == 0)
+    @pl.when(pc_send & carry)
+    def _():
+        pc_sent(pl.ds(0, NCH))
+
+    @pl.when(pc_send & jnp.logical_not(carry))
+    def _():
+        pc_sent(pl.ds(HALF, HALF))
+
+    @pl.when(late)
     def _():
         b0_copy().wait_send()
 

time: 86.2 us -> 83.3 us (0.966)
  Pallas kernels: 84.4 us -> 82.3 us
    pallas_call x1, Pallas kernels: 83.8 us -> 81.7 us  [fused(): pl.pallas_call(functools.partial(body, n, ntp, sizes), name='delta_states...]
where the time goes in v4:
time: 83.3 us; the launch traced here: 83 us
  Pallas kernels  82.3 us (99%)
    pallas_call x1, Pallas kernels, fused(): pl.pallas_call(functools.partial(body, n, ntp, sizes), name='delta_states...  81.7 us

profile of v4, /device:TPU:40, one launch (start us, length us, event | category | flops | bytes accessed | tf_op | source)
XLA Modules:
  0.0 83.0 jit_solution(18057995497417828245)
XLA Ops:
  0.6 81.7 %delta_states.1 = (bf16[2,4,128]{2,1,0:T(4,128)(2,1)S(1)}, f32[2,8]{1,0:T(2,128)S(1)}) custom-call(bf16[2,512,2048]{2,1,0:T(8,128)(2,1)} %x_hbm.1, bf16[2048,128]{1,0:T(8,128)(2,1)} %wk_hbm.1, bf16[2048,128]{1,0:T(8,128)(2,1)} %wv_hbm.1, bf16[8,2048]{1,0:T(8,128)(2,1)} %bitcast.11, f32[1,8]{1,0:T(1,128)} %bitcast.14, bf16[8,2048]{1,0:T(8,128)(2,1)} %bitcast.12, ...), custom_call_target="tpu_custom_call" | custom-call | tf_op jit(solution)/shard_map/delta_states/pallas_call | solution.py:622
  82.4 0.6 hand_over.1

commit v5 on v4

--- a/solution.py
+++ b/solution.py
@@ -17,7 +17,7 @@
 ROWS = 256
 HALF = DK // CH
 NCH = 2 * HALF
-GROUPS = (1, 1, 1, 1, 1, 2, 2, 2, 2, 2, 3, 4, 4, 5)
+GROUPS = (1, 1, 1, 1, 1, 2, 2, 2, 2, 2, 2, 2, 3, 4, 5)
 NT = (((1,), (1,)), ((), ()))
 
 

time: 83.3 us -> 82.3 us (0.988)
  Pallas kernels: 82.3 us -> 80.5 us
    pallas_call x1, Pallas kernels: 81.7 us -> 79.9 us  [fused(): pl.pallas_call(functools.partial(body, n, ntp, sizes), name='delta_states...]
where the time goes in v5:
time: 82.3 us; the launch traced here: 81.2 us
  Pallas kernels  80.5 us (98%)
    pallas_call x1, Pallas kernels, fused(): pl.pallas_call(functools.partial(body, n, ntp, sizes), name='delta_states...  79.9 us

profile of v5, /device:TPU:40, one launch (start us, length us, event | category | flops | bytes accessed | tf_op | source)
XLA Modules:
  0.0 81.2 jit_solution(3787176857150899595)
XLA Ops:
  0.6 79.9 %delta_states.1 = (bf16[2,4,128]{2,1,0:T(4,128)(2,1)S(1)}, f32[2,8]{1,0:T(2,128)S(1)}) custom-call(bf16[2,512,2048]{2,1,0:T(8,128)(2,1)} %x_hbm.1, bf16[2048,128]{1,0:T(8,128)(2,1)} %wk_hbm.1, bf16[2048,128]{1,0:T(8,128)(2,1)} %wv_hbm.1, bf16[8,2048]{1,0:T(8,128)(2,1)} %bitcast.11, f32[1,8]{1,0:T(1,128)} %bitcast.14, bf16[8,2048]{1,0:T(8,128)(2,1)} %bitcast.12, ...), custom_call_target="tpu_custom_call" | custom-call | tf_op jit(solution)/shard_map/delta_states/pallas_call | solution.py:622
  80.6 0.6 hand_over.1
